TPU v7x, 32 devices: a whole 2x2x4 slice. The times are simulated.
32 devices in a mesh: st: 16 (over z, y, x), tp: 2 (over core).
Axes of the slice: x: 2, y: 2, z: 4, core: 2. Of those that a mesh axis runs over, the one named last changes fastest.
Arguments:
- tokens: bfloat16 [16384, 2048], P('st', 'tp'), may hold values from -6 to 6
- passage_ids: int32 [256, 2], P('st'), may hold values from 0 to 255, as said below
- passage_store: bfloat16 [256, 64, 2048], P('st'), may hold values from -6 to 6
- norm_gain: bfloat16 [2048], replicated, may hold values from 0.099609375 to 1.8984375
- conv_value_weight: bfloat16 [2048, 1536], P(None, 'tp'), may hold values from -0.125 to 0.125
- conv_gate_weight: bfloat16 [2048, 1536], P(None, 'tp'), may hold values from -0.125 to 0.125
- conv_weight: bfloat16 [31, 1536], P(None, 'tp'), may hold values from -1 to 1
- ln_gain: bfloat16 [1536], P('tp'), may hold values from 0.099609375 to 1.8984375
- query_weight: bfloat16 [2048, 512], P(None, 'tp'), may hold values from -0.125 to 0.125
- query_gain: bfloat16 [512], P('tp'), may hold values from 0.5 to 10
- passage_gain: bfloat16 [2048], replicated, may hold values from 0.099609375 to 1.8984375
- key_weight: bfloat16 [2048, 512], P(None, 'tp'), may hold values from -0.125 to 0.125
- value_weight: bfloat16 [2048, 512], P(None, 'tp'), may hold values from -0.125 to 0.125
- key_gain: bfloat16 [512], P('tp'), may hold values from 0.5 to 10
- memory_gate: bfloat16 [512], P('tp'), may hold values from 0.29882812 to 1.5
- conv_out_weight: bfloat16 [1536, 2048], P('tp'), may hold values from -0.125 to 0.125
- memory_out_weight: bfloat16 [512, 2048], P('tp'), may hold values from -0.125 to 0.125
Outputs:
- layer_out: bfloat16 [16384, 2048], P(('st', 'tp'))
Inputs may be any that keep to these rules, and one draw needn't show every extreme that they name: The owner of passage p is p // 16. Among the 32 entries of the rows of passage_ids that lie on one index of st (aligned runs of 16 rows, that is the blocks of one index of st), no owner is named more than 4 times, and in every such run some owner is named exactly 4 times.
All inputs are finite; a program needn't handle non-finite values.
Results may differ from a plain program's by a relative error of at most 0.008.
The roundings to bfloat16 on the way count: a program that leaves them out, or rounds other values in their place, can miss the bound.
Values may be sent and summed in bfloat16 or wider, within the bound.
A program may use at most 192 MiB of HBM per device.

v0:
```python
import functools

import jax
import jax.numpy as jnp
from jax import lax
from jax.experimental import pallas as pl
from jax.experimental.pallas import tpu as pltpu
from jax.sharding import PartitionSpec as P

C_A = 1536
MEM_HD = 64
KW = 31
SEQS_DEV = 2


NORM_EPS = 1e-06
LAYER_EPS = 1e-05
VMEM_LIMIT = 60 * 1024 * 1024


def params():
    return pltpu.CompilerParams(
        dimension_semantics=("arbitrary",), vmem_limit_bytes=VMEM_LIMIT
    )


def head_norm(product, gain_row):
    lane = lax.broadcasted_iota(jnp.int32, product.shape, 1)
    squares = product * product
    scale = jnp.zeros_like(product)
    for head in range(product.shape[1] // MEM_HD):
        inside = (lane >= head * MEM_HD) & (lane < (head + 1) * MEM_HD)
        total = jnp.sum(jnp.where(inside, squares, 0.0), axis=-1, keepdims=True)
        scale = jnp.where(inside, lax.rsqrt(total * (1.0 / MEM_HD) + NORM_EPS), scale)
    return (product * scale * gain_row.astype(jnp.float32)).astype(jnp.bfloat16)


def dot32(left, right):
    return jnp.dot(left, right, preferred_element_type=jnp.float32)


def passage_kernel(rows_ref, gain_ref, key_w_ref, value_w_ref, key_gain_ref, out_ref):
    rows = rows_ref[...].astype(jnp.float32)
    factor = lax.rsqrt(jnp.mean(rows * rows, axis=-1, keepdims=True) + NORM_EPS)
    normed = (rows * factor * gain_ref[...].astype(jnp.float32)).astype(jnp.bfloat16)
    width = key_w_ref.shape[1]
    out_ref[:, :width] = head_norm(dot32(normed, key_w_ref[...]), key_gain_ref[...])
    out_ref[:, width:] = dot32(normed, value_w_ref[...]).astype(jnp.bfloat16)


def project_passages(rows, gain, key_weight, value_weight, key_gain):
    count, features = rows.shape
    width = key_weight.shape[1]
    tile = min(256, count)
    whole = lambda i: (0, 0)
    return pl.pallas_call(
        passage_kernel,
        grid=(count // tile,),
        in_specs=[
            pl.BlockSpec((tile, features), lambda i: (i, 0)),
            pl.BlockSpec((1, features), whole),
            pl.BlockSpec((features, width), whole),
            pl.BlockSpec((features, width), whole),
            pl.BlockSpec((1, width), whole),
        ],
        out_specs=pl.BlockSpec((tile, 2 * width), lambda i: (i, 0)),
        out_shape=jax.ShapeDtypeStruct((count, 2 * width), jnp.bfloat16),
        compiler_params=params(),
        cost_estimate=pl.CostEstimate(
            flops=4 * count * features * width, bytes_accessed=8 << 20, transcendentals=0
        ),
        name="project_passages",
    )(rows, gain[None, :], key_weight, value_weight, key_gain[None, :])


def token_kernel(
    index_ref,
    own_ref,
    other_ref,
    own_gain_ref,
    other_gain_ref,
    own_value_ref,
    other_value_ref,
    own_gate_ref,
    other_gate_ref,
    own_query_ref,
    other_query_ref,
    query_gain_ref,
    gated_ref,
    query_ref,
):
    own = own_ref[...].astype(jnp.float32)
    other = other_ref[...].astype(jnp.float32)
    total = jnp.sum(own * own, axis=-1, keepdims=True) + jnp.sum(
        other * other, axis=-1, keepdims=True
    )
    factor = lax.rsqrt(total * (0.5 / own.shape[1]) + NORM_EPS)
    own = (own * factor * own_gain_ref[...].astype(jnp.float32)).astype(jnp.bfloat16)
    other = (other * factor * other_gain_ref[...].astype(jnp.float32)).astype(jnp.bfloat16)
    query = dot32(own, own_query_ref[...]) + dot32(other, other_query_ref[...])
    query_ref[...] = head_norm(query, query_gain_ref[...])
    value = dot32(own, own_value_ref[...]) + dot32(other, other_value_ref[...])
    gate = dot32(own, own_gate_ref[...]) + dot32(other, other_gate_ref[...])
    gated_ref[...] = (value * jax.nn.sigmoid(gate)).astype(jnp.bfloat16)


def project_tokens(tp, own, other, gain, value_w, gate_w, query_w, query_gain):
    count, half = own.shape
    width, query_width = value_w.shape[1], query_w.shape[1]
    tile = min(256, count)
    rows = lambda i, s: (i, 0)
    mine = lambda i, s: (s[0], 0)
    theirs = lambda i, s: (1 - s[0], 0)
    return pl.pallas_call(
        token_kernel,
        grid_spec=pltpu.PrefetchScalarGridSpec(
            num_scalar_prefetch=1,
            grid=(count // tile,),
            in_specs=[
                pl.BlockSpec((tile, half), rows),
                pl.BlockSpec((tile, half), rows),
                pl.BlockSpec((1, half), lambda i, s: (0, s[0])),
                pl.BlockSpec((1, half), lambda i, s: (0, 1 - s[0])),
                pl.BlockSpec((half, width), mine),
                pl.BlockSpec((half, width), theirs),
                pl.BlockSpec((half, width), mine),
                pl.BlockSpec((half, width), theirs),
                pl.BlockSpec((half, query_width), mine),
                pl.BlockSpec((half, query_width), theirs),
                pl.BlockSpec((1, query_width), lambda i, s: (0, 0)),
            ],
            out_specs=[
                pl.BlockSpec((tile, width), rows),
                pl.BlockSpec((tile, query_width), rows),
            ],
        ),
        out_shape=(
            jax.ShapeDtypeStruct((count, width), jnp.bfloat16),
            jax.ShapeDtypeStruct((count, query_width), jnp.bfloat16),
        ),
        compiler_params=params(),
        cost_estimate=pl.CostEstimate(
            flops=4 * count * half * (2 * width + query_width),
            bytes_accessed=16 << 20,
            transcendentals=0,
        ),
        name="project_tokens",
    )(
        tp.reshape(1),
        own,
        other,
        gain[None, :],
        gain[None, :],
        value_w,
        value_w,
        gate_w,
        gate_w,
        query_w,
        query_w,
        query_gain[None, :],
    )


def attend_kernel(passes, slots_ref, query_ref, kv_ref, gate_ref, out_ref):
    width = query_ref.shape[1]
    heads = width // MEM_HD
    block = query_ref.shape[0] * passes // slots_ref.shape[0]
    head_of = lax.broadcasted_iota(jnp.int32, (heads * block, width), 1) // MEM_HD
    row_head = lax.broadcasted_iota(jnp.int32, (heads * block, width), 0) // block
    inside = head_of == row_head
    gate = jnp.tanh(gate_ref[...].astype(jnp.float32))

    @pl.loop(0, slots_ref.shape[0] // passes)
    def _(index):
        rows = pl.ds(pl.multiple_of(index * block, block), block)
        query = query_ref[rows, :]
        stacked = jnp.concatenate([query] * heads, axis=0)
        stacked = jnp.where(inside, stacked, jnp.zeros_like(stacked))
        read = [kv_ref[slots_ref[index * passes + part]] for part in range(passes)]
        keys = jnp.concatenate([part[:, :width] for part in read], axis=0)
        values = jnp.concatenate([part[:, width:] for part in read], axis=0)
        scores = lax.dot_general(
            stacked, keys, (((1,), (1,)), ((), ())), preferred_element_type=jnp.float32
        ) * MEM_HD ** (-0.5)
        expanded = jnp.exp(scores - jnp.max(scores, axis=-1, keepdims=True))
        weights = (expanded / jnp.sum(expanded, axis=-1, keepdims=True)).astype(jnp.bfloat16)
        mixed = jnp.where(inside, dot32(weights, values), 0.0)
        attended = mixed[:block]
        for head in range(1, heads):
            attended = attended + mixed[head * block : (head + 1) * block]
        out_ref[rows, :] = (attended * gate).astype(jnp.bfloat16)


def attend(slots, queries, received, gate, passes):
    vmem = pl.BlockSpec(memory_space=pltpu.VMEM)
    return pl.pallas_call(
        functools.partial(attend_kernel, passes),
        in_specs=[pl.BlockSpec(memory_space=pltpu.SMEM), vmem, vmem, vmem],
        out_specs=vmem,
        out_shape=jax.ShapeDtypeStruct(queries.shape, jnp.bfloat16),
        compiler_params=pltpu.CompilerParams(vmem_limit_bytes=VMEM_LIMIT),
        cost_estimate=pl.CostEstimate(
            flops=1 << 29, bytes_accessed=5 << 20, transcendentals=0
        ),
        name="attend",
    )(slots, queries, received, gate[None, :])


def body(
    tokens,
    passage_ids,
    passage_store,
    norm_gain,
    conv_value_weight,
    conv_gate_weight,
    conv_weight,
    ln_gain,
    query_weight,
    query_gain,
    passage_gain,
    key_weight,
    value_weight,
    key_gain,
    memory_gate,
    conv_out_weight,
    memory_out_weight,
):
    owner_count = lax.axis_size("st")
    tp = lax.axis_index("tp").astype(jnp.int32)
    swap = [(0, 1), (1, 0)]
    store_size, passage_len, feature_count = passage_store.shape
    flat_ids = passage_ids.reshape(-1)
    request_count = flat_ids.shape[0]
    most_each = max(1, 2 * request_count // owner_count)
    owner_index = flat_ids // store_size
    local_index = flat_ids % store_size
    owner_onehot = (
        owner_index[:, None] == jnp.arange(owner_count, dtype=jnp.int32)[None, :]
    ).astype(jnp.int32)
    earlier = jnp.cumsum(owner_onehot, axis=0) - owner_onehot
    slot_index = owner_index * most_each + jnp.sum(earlier * owner_onehot, axis=1)
    slot_onehot = (
        slot_index[:, None] == jnp.arange(owner_count * most_each, dtype=jnp.int32)[None, :]
    ).astype(jnp.int32)
    wanted = jnp.sum(slot_onehot * local_index[:, None], axis=0)
    asked_for = lax.all_to_all(
        wanted.reshape(owner_count, most_each), "st", split_axis=0, concat_axis=0, tiled=True
    ).reshape(-1)
    other_tokens = lax.ppermute(tokens, "tp", swap)
    projected = project_passages(
        passage_store.reshape(-1, feature_count), passage_gain, key_weight, value_weight, key_gain
    ).reshape(store_size, passage_len, -1)
    sent = jnp.take(projected, asked_for, axis=0, mode="clip")
    received = lax.all_to_all(sent, "st", split_axis=0, concat_axis=0, tiled=True)

    gated_rows, queries = project_tokens(
        tp,
        tokens,
        other_tokens,
        norm_gain,
        conv_value_weight,
        conv_gate_weight,
        query_weight,
        query_gain,
    )
    channel_count = conv_value_weight.shape[1]
    sequences = gated_rows.reshape(SEQS_DEV, -1, channel_count)
    filtered = lax.conv_general_dilated(
        sequences,
        conv_weight[:, None, :],
        (1,),
        [(KW - 1, 0)],
        dimension_numbers=("NWC", "WIO", "NWC"),
        feature_group_count=channel_count,
        preferred_element_type=jnp.float32,
    ).reshape(-1, channel_count)
    own_sums = jnp.stack([jnp.sum(filtered, axis=-1), jnp.sum(filtered * filtered, axis=-1)])
    stat_sums = own_sums + lax.ppermute(own_sums, "tp", swap)
    channel_mean = (stat_sums[0] / C_A)[:, None]
    channel_var = (stat_sums[1] / C_A)[:, None] - channel_mean * channel_mean
    scaled = (
        (filtered - channel_mean) * lax.rsqrt(channel_var + LAYER_EPS) * ln_gain.astype(jnp.float32)
    )
    conv_out = jax.nn.silu(scaled).astype(jnp.bfloat16)
    share = conv_out.shape[0] // 2
    conv_send = dot32(lax.dynamic_slice_in_dim(conv_out, (1 - tp) * share, share), conv_out_weight)
    conv_keep = dot32(lax.dynamic_slice_in_dim(conv_out, tp * share, share), conv_out_weight)

    memory = attend(slot_index, queries, received, memory_gate, passage_ids.shape[1])
    memory_send = lax.dynamic_slice_in_dim(memory, (1 - tp) * share, share)
    part_send = (conv_send + dot32(memory_send, memory_out_weight)).astype(jnp.bfloat16)
    part_back = lax.ppermute(part_send, "tp", swap)
    memory_keep = lax.dynamic_slice_in_dim(memory, tp * share, share)
    part_keep = (conv_keep + dot32(memory_keep, memory_out_weight)).astype(jnp.bfloat16)
    return (part_keep.astype(jnp.float32) + part_back.astype(jnp.float32)).astype(jnp.bfloat16)


def solution(mesh):
    return jax.shard_map(
        body,
        mesh=mesh,
        in_specs=(
            P("st", "tp"),
            P("st", None),
            P("st", None, None),
            P(),
            P(None, "tp"),
            P(None, "tp"),
            P(None, "tp"),
            P("tp"),
            P(None, "tp"),
            P("tp"),
            P(),
            P(None, "tp"),
            P(None, "tp"),
            P("tp"),
            P("tp"),
            P("tp", None),
            P("tp", None),
        ),
        out_specs=P(("st", "tp"), None),
        check_vma=False,
    )
```

profile of v0, /device:TPU:15, one launch (start us, length us, event | category | flops | bytes accessed | tf_op | source)
XLA Modules:
  0.0 149.9 jit_solution(2094496723277717775)
XLA Ops:
  0.0 0.9 copy.47
  1.4 0.7 all_to_all.9
  2.1 6.6 %all-to-all-start = ((s32[16,1,4]{2,1,0:T(1,128)}), s32[16,1,4]{2,1,0:T(1,128)S(1)}, u32[]{:S(2)}, u32[]{:S(2)}) async-start(s32[16,1,4]{2,1,0:T(1,128)} %bitcast.10), calls=%async_computation | async-start | bytes 16384 | tf_op jit(solution)/shard_map/all_to_all | solution.py:246
  8.7 1.2 broadcast_in_dim.35.key_gain_ref
  10.0 1.3 broadcast_in_dim.34.gain_ref
  11.2 7.2 %project_passages.1 = bf16[1024,512]{1,0:T(8,128)(2,1)} custom-call(bf16[1024,2048]{1,0:T(8,128)(2,1)} %bitcast.47, bf16[1,2048]{1,0:T(2,128)(2,1)} %broadcast_in_dim.34.gain_ref, bf16[2048,256]{1,0:T(8,128)(2,1)} %key_w_ref.1, bf16[2048,256]{1,0:T(8,128)(2,1)} %value_w_ref.1, bf16[1,256]{1,0:T(2,128)(2,1)} %broadcast_in_dim.35.key_gain_ref), custom_call_target="tpu_custom_call" | custom-call | flops 2147483648 | bytes 8388608 | tf_op jit(solution)/shard_map/project_passages/pallas_call | solution.py:56
  18.5 0.6 broadcast.152
  19.1 0.7 reduce.8
  19.9 4.0 %gather_fusion = bf16[64,64,512]{2,1,0:T(8,128)(2,1)} fusion(bf16[16,64,512]{2,1,0:T(8,128)(2,1)} %bitcast.36, s32[1024]{0:T(1024)S(1)} %pad_clamp_fusion), kind=kCustom, calls=%fused_computation | custom fusion | bytes 8388864 | tf_op jit(solution)/shard_map/jit(_take)/gather | solution.py:253
  23.9 6.5 %all-to-all-start.1 = ((bf16[64,64,512]{2,1,0:T(8,128)(2,1)}), bf16[64,64,512]{2,1,0:T(8,128)(2,1)}, u32[]{:S(2)}, u32[]{:S(2)}) async-start(bf16[64,64,512]{2,1,0:T(8,128)(2,1)} %gather_fusion), calls=%async_computation.1 | async-start | bytes 8388608 | tf_op jit(solution)/shard_map/all_to_all | solution.py:254
  30.4 1.8 %collective-permute-start = (bf16[1024,1024]{1,0:T(8,128)(2,1)}, bf16[1024,1024]{1,0:T(8,128)(2,1)}, u32[]{:S(2)}, u32[]{:S(2)}) collective-permute-start(bf16[1024,1024]{1,0:T(8,128)(2,1)} %own_ref.1), channel_id=1, source_target_pairs={{0,1},{1,0},{2,3},{3,2},{4,5},{5,4},{6,7},{7,6},{8,9},{9,8},{10,11... | collective-permute-start | bytes 6291464 | tf_op jit(solution)/shard_map/ppermute | solution.py:249
  32.2 0.6 broadcast_in_dim.32.query_gain_ref
  32.8 0.6 broadcast_in_dim.16.own_gain_ref.other_gain_ref
  33.4 2.9 %collective-permute-done.other_ref = bf16[1024,1024]{1,0:T(8,128)(2,1)} collective-permute-done((bf16[1024,1024]{1,0:T(8,128)(2,1)}, bf16[1024,1024]{1,0:T(8,128)(2,1)}, u32[]{:S(2)}, u32[]{:S(2)}) %collective-permute-start) | collective-permute-done | bytes 2097184 | tf_op jit(solution)/shard_map/ppermute | solution.py:249
  36.3 13.6 %project_tokens.1 = (bf16[1024,768]{1,0:T(8,128)(2,1)}, bf16[1024,256]{1,0:T(8,128)(2,1)}) custom-call(s32[1]{0:T(128)} %bitcast.index_ref, bf16[1024,1024]{1,0:T(8,128)(2,1)} %own_ref.1, bf16[1024,1024]{1,0:T(8,128)(2,1)} %collective-permute-done.other_ref, bf16[1,2048]{1,0:T(2,128)(2,1)} %broadcast_in_dim.16.own_gain_ref.other_gain_ref, ...), custom_call_target="tpu_custom_call" | custom-call | flops 7516192768 | bytes 16777216 | tf_op jit(solution)/shard_map/project_tokens/pallas_call | solution.py:114
  49.9 3.0 %copy.41 = bf16[2,512,768]{2,0,1:T(2,128)(2,1)S(1)} copy(bf16[2,512,768]{2,1,0:T(8,128)(2,1)} %bitcast.39) | data formatting | bytes 3145728 | tf_op jit(solution)/shard_map/reshape | solution.py:267
  52.9 1.3 pad
  54.7 7.0 %fusion.2 = bf16[2,8,98,768]{3,0,2,1:T(2,128)(2,1)S(1)} fusion(bf16[2,7,30,768]{3,0,2,1:T(2,128)(2,1)S(1)} %slice.14, bf16[2,8,68,768]{3,0,2,1:T(2,128)(2,1)S(1)} %bitcast.38), kind=kLoop, calls=%fused_computation.10 | loop fusion | flops 7225344 | bytes 4724736 | tf_op jit(solution)/shard_map/conv_general_dilated | solution.py:268
  61.7 11.5 %fusion.21 = (f32[16,68]{0,1:T(8,128)S(1)}, f32[16,68]{0,1:T(8,128)S(1)}, f32[16,68,768]{2,0,1:T(8,128)}) fusion(bf16[31,1,768]{2,0,1:T(8,128)(2,1)S(1)} %bitcast.48, bf16[2,8,98,768]{3,0,2,1:T(2,128)(2,1)S(1)} %fusion.2, pred[16,68]{0,1:T(8,128)(4,1)S(1)} %copy-done.10), kind=kOutput, calls=%fused_computation.45 | convolution fusion | flops 55146368 | bytes 5808192 | tf_op jit(solution)/shard_map/conv_general_dilated | solution.py:268
  74.7 5.7 %copy.44 = f32[16,68,768]{2,1,0:T(8,128)} copy(f32[16,68,768]{2,0,1:T(8,128)} %get-tuple-element.15) | data formatting | bytes 6684672 | tf_op jit(solution)/shard_map/conv_general_dilated | solution.py:268
  80.3 4.4 %reshape.129 = f32[2,544,768]{2,1,0:T(8,128)} reshape(f32[16,68,768]{2,1,0:T(8,128)} %copy.44) | data formatting | bytes 6684672 | tf_op jit(solution)/shard_map/conv_general_dilated | solution.py:268
  84.8 1.8 %slice-done = f32[2,512,768]{2,1,0:T(8,128)S(1)} async-done(((f32[2,544,768]{2,1,0:T(8,128)}), f32[2,512,768]{2,1,0:T(8,128)S(1)}, s32[]{:S(2)}) %slice-start) | async-done | bytes 3145752 | tf_op jit(solution)/shard_map/conv_general_dilated | solution.py:268
  86.6 1.0 multiply_convert_fusion
  87.6 1.2 copy-done.3
  88.8 3.8 %fusion.8 = f32[512,2048]{1,0:T(8,128)} fusion(bf16[768,2048]{1,0:T(8,128)(2,1)S(1)} %copy-done, bf16[1024,768]{1,0:T(8,128)(2,1)S(1)} %multiply_convert_fusion, s32[]{:T(128)S(6)} %select_n.34), kind=kOutput, calls=%fused_computation.15 | convolution fusion | flops 1610612736 | bytes 8126468 | tf_op jit(solution)/shard_map/dot_general | solution.py:39
  92.5 31.4 %all-to-all-done.1.kv_ref = bf16[64,64,512]{2,1,0:T(8,128)(2,1)} async-done(((bf16[64,64,512]{2,1,0:T(8,128)(2,1)}), bf16[64,64,512]{2,1,0:T(8,128)(2,1)}, u32[]{:S(2)}, u32[]{:S(2)}) %all-to-all-start.1) | async-done | bytes 4194336 | tf_op jit(solution)/shard_map/all_to_all | solution.py:254
  124.0 12.0 %attend.1 = bf16[1024,256]{1,0:T(8,128)(2,1)} custom-call(s32[32]{0:T(128)} %copy-done.6, bf16[1024,256]{1,0:T(8,128)(2,1)} %get-tuple-element.8.query_ref, bf16[64,64,512]{2,1,0:T(8,128)(2,1)} %all-to-all-done.1.kv_ref, bf16[1,256]{1,0:T(2,128)(2,1)} %broadcast_in_dim.37.gate_ref), custom_call_target="tpu_custom_call" | custom-call | flops 536870912 | bytes 5242880 | tf_op jit(solution)/shard_map/attend/pallas_call | solution.py:196
  136.0 4.6 %add_convert_fusion.1 = bf16[512,2048]{1,0:T(8,128)(2,1)} fusion(f32[512,2048]{1,0:T(8,128)} %fusion.8, bf16[256,2048]{1,0:T(8,128)(2,1)} %param.33, bf16[1024,256]{1,0:T(8,128)(2,1)} %attend.1, s32[]{:T(128)S(6)} %select_n.34), kind=kOutput, calls=%fused_computation.3 | convolution fusion | flops 538968064 | bytes 7602180 | tf_op jit(solution)/shard_map/dot_general | solution.py:39
  140.6 1.4 collective-permute-start.2
  142.1 3.0 %fusion.10 = f32[512,2048]{1,0:T(8,128)S(1)} fusion(bf16[768,2048]{1,0:T(8,128)(2,1)S(1)} %copy-done, bf16[1024,768]{1,0:T(8,128)(2,1)} %copy-done.3, s32[]{:T(128)S(6)} %select_n.31), kind=kOutput, calls=%fused_computation.17 | convolution fusion | flops 1610612736 | bytes 8126468 | tf_op jit(solution)/shard_map/dot_general | solution.py:39
  145.1 1.1 collective-permute-done.2
  146.2 3.7 %add_convert_fusion = bf16[512,2048]{1,0:T(8,128)(2,1)} fusion(bf16[512,2048]{1,0:T(8,128)(2,1)} %collective-permute-done.2, f32[512,2048]{1,0:T(8,128)S(1)} %fusion.10, bf16[256,2048]{1,0:T(8,128)(2,1)S(1)} %copy-done.1, bf16[1024,256]{1,0:T(8,128)(2,1)S(1)} %copy-done.2, s32[]{:T(128)S(6)} %select_n.31), kind=kOutput, calls=%fused_computation.2 | convolution fusion | flops 543162368 | bytes 9699332 | tf_op jit(solution)/shard_map/dot_general | solution.py:39
  (49 shorter events, 2.5 us)
Async XLA Ops:
  0.0 88.8 %copy-start = (bf16[768,2048]{1,0:T(8,128)(2,1)S(1)}, bf16[768,2048]{1,0:T(8,128)(2,1)}, u32[]{:S(2)}) copy-start(bf16[768,2048]{1,0:T(8,128)(2,1)} %param.32) | copy-start | bytes 9437188
  1.3 17.1 %copy-start.6 = (s32[32]{0:T(128)}, s32[32]{0:T(128)S(1)}, u32[]{:S(2)}) copy-start(s32[32]{0:T(128)S(1)} %multiply_add_fusion.slots_ref) | copy-start | bytes 388
  2.1 16.3 %all-to-all-start = ((s32[16,1,4]{2,1,0:T(1,128)}), s32[16,1,4]{2,1,0:T(1,128)S(1)}, u32[]{:S(2)}, u32[]{:S(2)}) async-start(s32[16,1,4]{2,1,0:T(1,128)} %bitcast.10), calls=%async_computation | async-start | bytes 16384 | tf_op jit(solution)/shard_map/all_to_all | solution.py:246
  23.9 8.3 %copy-start.8 = (bf16[256]{0:T(256)(128)(2,1)S(1)}, bf16[256]{0:T(256)(128)(2,1)}, u32[]{:S(2)}) copy-start(bf16[256]{0:T(256)(128)(2,1)} %param.26) | copy-start | bytes 1540
  23.9 8.9 %copy-start.4 = (bf16[2048]{0:T(1024)(128)(2,1)S(1)}, bf16[2048]{0:T(1024)(128)(2,1)}, u32[]{:S(2)}) copy-start(bf16[2048]{0:T(1024)(128)(2,1)} %param.20) | copy-start | bytes 12292
  23.9 100.1 %all-to-all-start.1 = ((bf16[64,64,512]{2,1,0:T(8,128)(2,1)}), bf16[64,64,512]{2,1,0:T(8,128)(2,1)}, u32[]{:S(2)}, u32[]{:S(2)}) async-start(bf16[64,64,512]{2,1,0:T(8,128)(2,1)} %gather_fusion), calls=%async_computation.1 | async-start | bytes 8388608 | tf_op jit(solution)/shard_map/all_to_all | solution.py:254
  30.4 5.9 %collective-permute-start = (bf16[1024,1024]{1,0:T(8,128)(2,1)}, bf16[1024,1024]{1,0:T(8,128)(2,1)}, u32[]{:S(2)}, u32[]{:S(2)}) collective-permute-start(bf16[1024,1024]{1,0:T(8,128)(2,1)} %own_ref.1), channel_id=1, source_target_pairs={{0,1},{1,0},{2,3},{3,2},{4,5},{5,4},{6,7},{7,6},{8,9},{9,8},{10,11... | collective-permute-start | bytes 6291464 | tf_op jit(solution)/shard_map/ppermute | solution.py:249
  54.2 7.5 %copy-start.7 = (bf16[31,768]{1,0:T(8,128)(2,1)S(1)}, bf16[31,768]{1,0:T(8,128)(2,1)}, u32[]{:S(2)}) copy-start(bf16[31,768]{1,0:T(8,128)(2,1)} %param.23) | copy-start | bytes 142852
  54.2 7.5 %copy-start.10 = (pred[16,68]{0,1:T(8,128)(4,1)S(1)}, pred[16,68]{0,1:T(8,128)(4,1)}, u32[]{:S(2)}) copy-start(pred[16,68]{0,1:T(8,128)(4,1)} %constant.61) | copy-start | bytes 3268
  61.7 12.4 %copy-start.9 = (bf16[256]{0:T(256)(128)(2,1)S(1)}, bf16[256]{0:T(256)(128)(2,1)}, u32[]{:S(2)}) copy-start(bf16[256]{0:T(256)(128)(2,1)} %param.31) | copy-start | bytes 1540
  61.7 12.9 %copy-start.5 = (bf16[768]{0:T(1024)(128)(2,1)S(1)}, bf16[768]{0:T(1024)(128)(2,1)}, u32[]{:S(2)}) copy-start(bf16[768]{0:T(1024)(128)(2,1)} %param.24) | copy-start | bytes 4612
  73.7 11.0 %collective-permute-start.1 = (f32[2,1024]{1,0:T(2,128)S(1)}, f32[2,1024]{1,0:T(2,128)S(1)}, u32[]{:S(2)}, u32[]{:S(2)}) collective-permute-start(f32[2,1024]{1,0:T(2,128)S(1)} %pad_maximum_fusion), channel_id=1, source_target_pairs={{0,1},{1,0},{2,3},{3,2},{4,5},{5,4},{6,7},{7,6},{8,9},{9,8},{10,11... | collective-permute-start | bytes 24584 | tf_op jit(solution)/shard_map/ppermute | solution.py:278
  84.7 1.9 %slice-start = ((f32[2,544,768]{2,1,0:T(8,128)}), f32[2,512,768]{2,1,0:T(8,128)S(1)}, s32[]{:S(2)}) async-start(f32[2,544,768]{2,1,0:T(8,128)} %reshape.129), calls=%async_computation.2 | async-start | bytes 6291456 | tf_op jit(solution)/shard_map/conv_general_dilated | solution.py:268
  87.6 1.2 copy-start.3
  140.6 5.5 %collective-permute-start.2 = (bf16[512,2048]{1,0:T(8,128)(2,1)}, bf16[512,2048]{1,0:T(8,128)(2,1)}, u32[]{:S(2)}, u32[]{:S(2)}) collective-permute-start(bf16[512,2048]{1,0:T(8,128)(2,1)} %add_convert_fusion.1), channel_id=1, source_target_pairs={{0,1},{1,0},{2,3},{3,2},{4,5},{5,4},{6,7},{7,6},{8,9},{9,8},{10,11... | collective-permute-start | bytes 6291464 | tf_op jit(solution)/shard_map/ppermute | solution.py:292
  142.0 4.1 %copy-start.1 = (bf16[256,2048]{1,0:T(8,128)(2,1)S(1)}, bf16[256,2048]{1,0:T(8,128)(2,1)}, u32[]{:S(2)}) copy-start(bf16[256,2048]{1,0:T(8,128)(2,1)} %param.33) | copy-start | bytes 3145732
  142.1 4.1 %copy-start.2 = (bf16[1024,256]{1,0:T(8,128)(2,1)S(1)}, bf16[1024,256]{1,0:T(8,128)(2,1)}, u32[]{:S(2)}) copy-start(bf16[1024,256]{1,0:T(8,128)(2,1)} %attend.1) | copy-start | bytes 1572868
where the time goes:
time: 151 us; the launch traced here: 150 us
  waiting for transfers between devices  35.5 us (24%)
  Pallas kernels  32.8 us (22%)
  local copies, waits for them, and re-layouts  28.8 us (19%)
  matrix products  26.7 us (18%)
  starting transfers between devices  16.7 us (11%)
  other arithmetic  9.15 us (6%)
    all_to_all x1, waiting for transfers between devices, body(): lax.all_to_all(sent, 'st', split_axis=0, concat_axis=0, tiled=True)  31.4 us
    dot_general x4, matrix products, dot32(): return jnp.dot(left, right, preferred_element_type=jnp.float32)  15.2 us
    pallas_call x1, Pallas kernels, project_tokens(): pl.pallas_call(token_kernel, grid_spec=pltpu.PrefetchScalarGridSpec(num_s...  13.6 us
    conv_general_dilated x5, local copies, waits for them, and re-layouts, body(): lax.conv_general_dilated(sequences, conv_weight[:, None, :], (1,), [(KW -...  12.3 us
    pallas_call x1, Pallas kernels, attend(): pl.pallas_call(functools.partial(attend_kernel, passes), in_specs=[pl.Blo...  12 us
    conv_general_dilated x1, matrix products, body(): lax.conv_general_dilated(sequences, conv_weight[:, None, :], (1,), [(KW -...  11.5 us
    pallas_call x1, Pallas kernels, project_passages(): pl.pallas_call(passage_kernel, grid=(count // tile,), in_specs=[pl.BlockS...  7.23 us
    conv_general_dilated x1, other arithmetic, body(): lax.conv_general_dilated(sequences, conv_weight[:, None, :], (1,), [(KW -...  7 us
  transfers between devices with their start and end apart: 5, of which 3 were waited for; matrix products, arithmetic and copies ran while one was open for 31% of the time, Pallas kernels for 14%

commit v1 on v0

--- a/solution.py
+++ b/solution.py
@@ -7,15 +7,15 @@
 from jax.experimental.pallas import tpu as pltpu
 from jax.sharding import PartitionSpec as P
 
+
 C_A = 1536
 MEM_HD = 64
-KW = 31
 SEQS_DEV = 2
 
 
 NORM_EPS = 1e-06
 LAYER_EPS = 1e-05
-VMEM_LIMIT = 60 * 1024 * 1024
+VMEM_LIMIT = 48 * 1024 * 1024
 
 
 def params():
@@ -161,7 +161,109 @@
     )
 
 
-def attend_kernel(passes, slots_ref, query_ref, kv_ref, gate_ref, out_ref):
+def pick_kernel(most, stages, halves, *refs):
+    asked_ref, refs = refs[0], refs[1:]
+    count = halves if halves else len(stages)
+    blocks, outs = refs[:count], refs[count:]
+    for mate, out_ref in enumerate(outs):
+        for place, relative in enumerate(stages):
+            for slot in range(most):
+                wanted = asked_ref[mate, relative * most + slot]
+                target = place * most + slot
+                if halves:
+                    split = blocks[0].shape[0]
+
+                    @pl.when(wanted < split)
+                    def _():
+                        out_ref[target] = blocks[0][jnp.minimum(wanted, split - 1)]
+
+                    @pl.when(wanted >= split)
+                    def _():
+                        out_ref[target] = blocks[1][jnp.maximum(wanted - split, 0)]
+
+                else:
+                    out_ref[target] = blocks[place][wanted]
+
+
+def pick(asked, blocks, stages, halves, most):
+    vmem = pl.BlockSpec(memory_space=pltpu.VMEM)
+    mates = asked.shape[0]
+    shape = (len(stages) * most,) + blocks[0].shape[1:]
+    return pl.pallas_call(
+        functools.partial(pick_kernel, most, stages, len(blocks) if halves else 0),
+        in_specs=[pl.BlockSpec(memory_space=pltpu.SMEM)] + [vmem] * len(blocks),
+        out_specs=[vmem] * mates,
+        out_shape=[jax.ShapeDtypeStruct(shape, jnp.bfloat16)] * mates,
+        compiler_params=pltpu.CompilerParams(vmem_limit_bytes=16 << 20),
+        cost_estimate=pl.CostEstimate(
+            flops=1 << 28, bytes_accessed=2 << 20, transcendentals=0
+        ),
+        name="pick",
+    )(asked, *blocks)
+
+
+def conv_kernel(rows_ref, taps_ref, out_ref, padded_ref):
+    length, width = rows_ref.shape
+    taps = taps_ref.shape[0]
+    lead = -(-(taps - 1) // 8) * 8
+    chunk = 64
+    span = chunk + lead + 8
+    padded_ref[:lead, :] = jnp.zeros((lead, width), jnp.float32)
+    padded_ref[lead + length :, :] = jnp.zeros((8, width), jnp.float32)
+    padded_ref[lead : lead + length, :] = rows_ref[...].astype(jnp.float32)
+    weights = taps_ref[...].astype(jnp.float32)
+
+    @pl.loop(0, length // chunk)
+    def _(index):
+        base = pl.multiple_of(index * chunk, chunk)
+        window = padded_ref[pl.ds(base, span), :]
+        total = jnp.zeros((chunk, width), jnp.float32)
+        for shift in range(8):
+            moved = window if shift == 0 else pltpu.roll(window, span - shift, 0)
+            for start in range(0, lead + 1, 8):
+                tap = start + shift - (lead - taps + 1)
+                if 0 <= tap < taps:
+                    total += weights[tap : tap + 1, :] * moved[start : start + chunk, :]
+        out_ref[pl.ds(base, chunk), :] = total
+
+
+def depthwise(rows, taps, sequences):
+    count, channels = rows.shape
+    length = count // sequences
+    width = 256 if channels % 256 == 0 else channels
+    lead = -(-(taps.shape[0] - 1) // 8) * 8
+    return pl.pallas_call(
+        conv_kernel,
+        grid=(sequences, channels // width),
+        in_specs=[
+            pl.BlockSpec((length, width), lambda i, j: (i, j)),
+            pl.BlockSpec((taps.shape[0], width), lambda i, j: (0, j)),
+        ],
+        out_specs=pl.BlockSpec((length, width), lambda i, j: (i, j)),
+        out_shape=jax.ShapeDtypeStruct(rows.shape, jnp.float32),
+        scratch_shapes=[pltpu.VMEM((lead + length + 8, width), jnp.float32)],
+        compiler_params=pltpu.CompilerParams(
+            dimension_semantics=("arbitrary", "arbitrary"), vmem_limit_bytes=16 << 20
+        ),
+        cost_estimate=pl.CostEstimate(
+            flops=8 << 30, bytes_accessed=5 << 20, transcendentals=0
+        ),
+        name="depthwise",
+    )(rows, taps)
+
+
+def attend_kernel(passes, most, plan, slots_ref, query_ref, gate_ref, *refs):
+    pieces, (out_ref, kv_ref, sems) = refs[:-3], refs[-3:]
+    copies = []
+    for number, (piece, start, slot) in enumerate(plan):
+        copies.append(
+            pltpu.make_async_copy(
+                pieces[piece].at[pl.ds(start, most)],
+                kv_ref.at[pl.ds(slot, most)],
+                sems.at[number],
+            )
+        )
+        copies[-1].start()
     width = query_ref.shape[1]
     heads = width // MEM_HD
     block = query_ref.shape[0] * passes // slots_ref.shape[0]
@@ -169,8 +271,10 @@
     row_head = lax.broadcasted_iota(jnp.int32, (heads * block, width), 0) // block
     inside = head_of == row_head
     gate = jnp.tanh(gate_ref[...].astype(jnp.float32))
-
-    @pl.loop(0, slots_ref.shape[0] // passes)
+    for copy in copies:
+        copy.wait()
+
+    @pl.loop(0, slots_ref.shape[0] // passes, unroll=4)
     def _(index):
         rows = pl.ds(pl.multiple_of(index * block, block), block)
         query = query_ref[rows, :]
@@ -191,22 +295,36 @@
         out_ref[rows, :] = (attended * gate).astype(jnp.bfloat16)
 
 
-def attend(slots, queries, received, gate, passes):
+def attend(slots, queries, pieces, plan, most, gate, passes):
     vmem = pl.BlockSpec(memory_space=pltpu.VMEM)
+    anywhere = pl.BlockSpec(memory_space=pl.ANY)
     return pl.pallas_call(
-        functools.partial(attend_kernel, passes),
-        in_specs=[pl.BlockSpec(memory_space=pltpu.SMEM), vmem, vmem, vmem],
+        functools.partial(attend_kernel, passes, most, plan),
+        in_specs=[pl.BlockSpec(memory_space=pltpu.SMEM), vmem, vmem]
+        + [anywhere] * len(pieces),
         out_specs=vmem,
         out_shape=jax.ShapeDtypeStruct(queries.shape, jnp.bfloat16),
-        compiler_params=pltpu.CompilerParams(vmem_limit_bytes=VMEM_LIMIT),
+        scratch_shapes=[
+            pltpu.VMEM((len(plan) * most,) + pieces[0].shape[1:], jnp.bfloat16),
+            pltpu.SemaphoreType.DMA((len(plan),)),
+        ],
+        compiler_params=pltpu.CompilerParams(vmem_limit_bytes=24 << 20),
         cost_estimate=pl.CostEstimate(
             flops=1 << 29, bytes_accessed=5 << 20, transcendentals=0
         ),
         name="attend",
-    )(slots, queries, received, gate[None, :])
-
-
-def body(
+    )(slots, queries, gate[None, :], *pieces)
+
+
+def split_axis(count):
+    plane = 1
+    for size in range(1, count + 1):
+        if count % size == 0 and size * size <= count:
+            plane = size
+    return count // plane, plane
+
+
+def layer(
     tokens,
     passage_ids,
     passage_store,
@@ -226,32 +344,64 @@
     memory_out_weight,
 ):
     owner_count = lax.axis_size("st")
+    me = lax.axis_index("st").astype(jnp.int32)
     tp = lax.axis_index("tp").astype(jnp.int32)
     swap = [(0, 1), (1, 0)]
+    depth, plane = split_axis(owner_count)
+    power = plane & (plane - 1) == 0
     store_size, passage_len, feature_count = passage_store.shape
+
+    def mate_of(place, step):
+        return place ^ step if power else (place + step) % plane
+
+    def along_plane(value, step, back):
+        pairs = [
+            (z * plane + p, z * plane + mate_of(p, step))
+            for z in range(depth)
+            for p in range(plane)
+        ]
+        return lax.ppermute(value, "st", [(b, a) for a, b in pairs] if back else pairs)
+
+    def along_depth(value, step):
+        pairs = [(i, (i + step * plane) % owner_count) for i in range(owner_count)]
+        return lax.ppermute(value, "st", pairs)
+
+    other_tokens = lax.ppermute(tokens, "tp", swap)
+    own_block = project_passages(
+        passage_store.reshape(-1, feature_count), passage_gain, key_weight, value_weight, key_gain
+    ).reshape(store_size, passage_len, -1)
+
     flat_ids = passage_ids.reshape(-1)
     request_count = flat_ids.shape[0]
     most_each = max(1, 2 * request_count // owner_count)
     owner_index = flat_ids // store_size
     local_index = flat_ids % store_size
-    owner_onehot = (
-        owner_index[:, None] == jnp.arange(owner_count, dtype=jnp.int32)[None, :]
-    ).astype(jnp.int32)
-    earlier = jnp.cumsum(owner_onehot, axis=0) - owner_onehot
-    slot_index = owner_index * most_each + jnp.sum(earlier * owner_onehot, axis=1)
+    same = (owner_index[:, None] == owner_index[None, :]) & (
+        jnp.arange(request_count)[:, None] > jnp.arange(request_count)[None, :]
+    )
+    rank = jnp.sum(same.astype(jnp.int32), axis=1)
+    relative = (owner_index // plane - me // plane + depth) % depth
+    mate_place, my_place = owner_index % plane, me % plane
+    step_to = (mate_place ^ my_place) if power else (my_place - mate_place + plane) % plane
+    slot_index = (relative * plane + step_to) * most_each + rank
     slot_onehot = (
         slot_index[:, None] == jnp.arange(owner_count * most_each, dtype=jnp.int32)[None, :]
     ).astype(jnp.int32)
-    wanted = jnp.sum(slot_onehot * local_index[:, None], axis=0)
-    asked_for = lax.all_to_all(
-        wanted.reshape(owner_count, most_each), "st", split_axis=0, concat_axis=0, tiled=True
-    ).reshape(-1)
-    other_tokens = lax.ppermute(tokens, "tp", swap)
-    projected = project_passages(
-        passage_store.reshape(-1, feature_count), passage_gain, key_weight, value_weight, key_gain
-    ).reshape(store_size, passage_len, -1)
-    sent = jnp.take(projected, asked_for, axis=0, mode="clip")
-    received = lax.all_to_all(sent, "st", split_axis=0, concat_axis=0, tiled=True)
+    wanted = jnp.sum(slot_onehot * local_index[:, None], axis=0).reshape(depth, plane, most_each)
+    asked = jnp.stack(
+        [wanted[:, 0]] + [along_plane(wanted[:, step], step, True) for step in range(1, plane)]
+    ).reshape(plane, depth * most_each)
+
+    pieces, plan = [], []
+
+    def deliver(blocks, stages, halves):
+        picked = pick(asked, blocks, stages, halves, most_each)
+        for step, part in enumerate(picked):
+            for place, offset in enumerate(stages):
+                plan.append(
+                    (len(pieces), place * most_each, (offset * plane + step) * most_each)
+                )
+            pieces.append(part if step == 0 else along_plane(part, step, False))
 
     gated_rows, queries = project_tokens(
         tp,
@@ -263,17 +413,16 @@
         query_weight,
         query_gain,
     )
-    channel_count = conv_value_weight.shape[1]
-    sequences = gated_rows.reshape(SEQS_DEV, -1, channel_count)
-    filtered = lax.conv_general_dilated(
-        sequences,
-        conv_weight[:, None, :],
-        (1,),
-        [(KW - 1, 0)],
-        dimension_numbers=("NWC", "WIO", "NWC"),
-        feature_group_count=channel_count,
-        preferred_element_type=jnp.float32,
-    ).reshape(-1, channel_count)
+    asked, gated_rows = lax.optimization_barrier((asked, gated_rows))
+    deliver((own_block,), (0,), False)
+    pieces[0], gated_rows = lax.optimization_barrier((pieces[0], gated_rows))
+    filtered = depthwise(gated_rows, conv_weight, SEQS_DEV)
+
+    rising, falling = own_block, own_block
+    for hop in range(1, (depth - 1) // 2 + 1):
+        rising, falling = along_depth(rising, 1), along_depth(falling, -1)
+        rising, falling, filtered = lax.optimization_barrier((rising, falling, filtered))
+        deliver((rising, falling), (depth - hop, hop), False)
     own_sums = jnp.stack([jnp.sum(filtered, axis=-1), jnp.sum(filtered * filtered, axis=-1)])
     stat_sums = own_sums + lax.ppermute(own_sums, "tp", swap)
     channel_mean = (stat_sums[0] / C_A)[:, None]
@@ -285,8 +434,15 @@
     share = conv_out.shape[0] // 2
     conv_send = dot32(lax.dynamic_slice_in_dim(conv_out, (1 - tp) * share, share), conv_out_weight)
     conv_keep = dot32(lax.dynamic_slice_in_dim(conv_out, tp * share, share), conv_out_weight)
-
-    memory = attend(slot_index, queries, received, memory_gate, passage_ids.shape[1])
+    if depth % 2 == 0:
+        half = store_size // 2
+        low, high = along_depth(rising[:half], 1), along_depth(falling[half:], -1)
+        low, high, conv_send = lax.optimization_barrier((low, high, conv_send))
+        deliver((low, high), (depth // 2,), True)
+
+    memory = attend(
+        slot_index, queries, pieces, tuple(plan), most_each, memory_gate, passage_ids.shape[1]
+    )
     memory_send = lax.dynamic_slice_in_dim(memory, (1 - tp) * share, share)
     part_send = (conv_send + dot32(memory_send, memory_out_weight)).astype(jnp.bfloat16)
     part_back = lax.ppermute(part_send, "tp", swap)
@@ -297,7 +453,7 @@
 
 def solution(mesh):
     return jax.shard_map(
-        body,
+        layer,
         mesh=mesh,
         in_specs=(
             P("st", "tp"),

time: 151 us -> 143 us (0.947)
  matrix products: 26.7 us -> 6.32 us
  waiting for transfers between devices: 35.5 us -> 54.9 us
  local copies, waits for them, and re-layouts: 28.8 us -> 10.5 us
  Pallas kernels: 32.8 us -> 39.6 us
  starting transfers between devices: 16.7 us -> 22.2 us
  other arithmetic: 9.15 us -> 7.45 us
    ppermute x3 -> x19, waiting for transfers between devices: 4 us -> 54.9 us  [the longest x4 30.2 us: along_depth(): return lax.ppermute(value, 'st', pairs)]
    all_to_all x2 -> x0, waiting for transfers between devices: 31.5 us -> none  [the longest x1 31.4 us: body(): lax.all_to_all(sent, 'st', split_axis=0, concat_axis=0, tiled=True)]
    ppermute x3 -> x19, starting transfers between devices: 3.61 us -> 22.2 us  [the longest x12 8.9 us: along_plane(): lax.ppermute(value, 'st', [(b, a) for a, b in pairs] if back else pairs)]
    all_to_all x2 -> x0, starting transfers between devices: 13.1 us -> none  [the longest x1 6.58 us: body(): lax.all_to_all(wanted.reshape(owner_count, most_each), 'st', split_axis=0...]
    conv_general_dilated x5 -> x0, local copies, waits for them, and re-layouts: 12.3 us -> none  [body(): lax.conv_general_dilated(sequences, conv_weight[:, None, :], (1,), [(KW -...]
    conv_general_dilated x1 -> x0, matrix products: 11.5 us -> none  [body(): lax.conv_general_dilated(sequences, conv_weight[:, None, :], (1,), [(KW -...]
    dot_general x4, matrix products: 15.2 us -> 6.32 us  [dot32(): return jnp.dot(left, right, preferred_element_type=jnp.float32)]
    pallas_call x1 -> x5, Pallas kernels: 12 us -> 20.4 us  [the longest x1 10.8 us: depthwise(): pl.pallas_call(conv_kernel, grid=(sequences, channels // width), in_specs...]
  transfers between devices with their start and end apart: 5 -> 19, of which waited for: 3 -> 10; matrix products, arithmetic and copies ran while one was open for 31% -> 8% of each run, Pallas kernels for 14% -> 24%
where the time goes in v1:
time: 143 us; the launch traced here: 141 us
  waiting for transfers between devices  54.9 us (38%)
  Pallas kernels  39.6 us (28%)
  starting transfers between devices  22.2 us (16%)
  local copies, waits for them, and re-layouts  10.5 us (7%)
  other arithmetic  7.45 us (5%)
  matrix products  6.32 us (4%)
    ppermute x4, waiting for transfers between devices, along_depth(): return lax.ppermute(value, 'st', pairs)  30.2 us
    ppermute x12, waiting for transfers between devices, along_plane(): lax.ppermute(value, 'st', [(b, a) for a, b in pairs] if back else pairs)  24.4 us
    pallas_call x1, Pallas kernels, project_tokens(): pl.pallas_call(token_kernel, grid_spec=pltpu.PrefetchScalarGridSpec(num_s...  12.5 us
    pallas_call x1, Pallas kernels, depthwise(): pl.pallas_call(conv_kernel, grid=(sequences, channels // width), in_specs...  10.8 us
    ppermute x12, starting transfers between devices, along_plane(): lax.ppermute(value, 'st', [(b, a) for a, b in pairs] if back else pairs)  8.9 us
    ppermute x1, starting transfers between devices, layer(): part_back = lax.ppermute(part_send, 'tp', swap)  8.72 us
    pallas_call x1, Pallas kernels, project_passages(): pl.pallas_call(passage_kernel, grid=(count // tile,), in_specs=[pl.BlockS...  6.67 us
    dot_general x4, matrix products, dot32(): return jnp.dot(left, right, preferred_element_type=jnp.float32)  6.32 us
  transfers between devices with their start and end apart: 19, of which 10 were waited for; matrix products, arithmetic and copies ran while one was open for 8% of the time, Pallas kernels for 24%

profile of v1, /device:TPU:15, one launch (start us, length us, event | category | flops | bytes accessed | tf_op | source)
XLA Modules:
  0.0 141.2 jit_solution(15343356248664237074)
XLA Ops:
  2.3 1.2 copy-done.4
  3.5 1.2 copy-done.5
  4.8 6.7 %project_passages.1 = bf16[1024,512]{1,0:T(8,128)(2,1)} custom-call(bf16[1024,2048]{1,0:T(8,128)(2,1)} %bitcast.24, bf16[1,2048]{1,0:T(2,128)(2,1)S(1)} %broadcast_in_dim.10.gain_ref, bf16[2048,256]{1,0:T(8,128)(2,1)S(1)} %copy-done.4, bf16[2048,256]{1,0:T(8,128)(2,1)S(1)} %copy-done.5, bf16[1,256]{1,0:T(2,128)(2,1)S(1)} %broadcast_in_dim.11.key_gain_ref), custom_call_target="tpu_custom_call" | custom-call | flops 2147483648 | bytes 8388608 | tf_op jit(solution)/shard_map/project_passages/pallas_call | solution.py:56
  11.6 1.3 collective-permute-start
  13.8 1.2 collective-permute-start.3
  15.2 1.8 %collective-permute-done.4 = s32[4,4]{1,0:T(4,128)S(1)} collective-permute-done((s32[4,4]{1,0:T(4,128)S(1)}, s32[4,4]{1,0:T(4,128)S(1)}, u32[]{:S(2)}, u32[]{:S(2)}) %collective-permute-start.4) | collective-permute-done | bytes 96 | tf_op jit(solution)/shard_map/ppermute | solution.py:363
  17.4 2.4 %collective-permute-done.2 = s32[4,4]{1,0:T(4,128)S(1)} collective-permute-done((s32[4,4]{1,0:T(4,128)S(1)}, s32[4,4]{1,0:T(4,128)S(1)}, u32[]{:S(2)}, u32[]{:S(2)}) %collective-permute-start.2) | collective-permute-done | bytes 96 | tf_op jit(solution)/shard_map/ppermute | solution.py:363
  19.9 1.6 %copy-done.3 = bf16[1024,1024]{1,0:T(8,128)(2,1)S(1)} copy-done((bf16[1024,1024]{1,0:T(8,128)(2,1)S(1)}, bf16[1024,1024]{1,0:T(8,128)(2,1)}, u32[]{:S(2)}) %copy-start.3) | copy-done | bytes 2097176
  21.5 1.2 copy-done.6
  22.7 12.5 %project_tokens.1 = (bf16[1024,768]{1,0:T(8,128)(2,1)S(1)}, bf16[1024,256]{1,0:T(8,128)(2,1)S(1)}) custom-call(s32[1]{0:T(128)} %bitcast.5.index_ref, bf16[1024,1024]{1,0:T(8,128)(2,1)S(1)} %copy-done.3, bf16[1024,1024]{1,0:T(8,128)(2,1)} %collective-permute-done.5.other_ref, bf16[1,2048]{1,0:T(2,128)(2,1)S(1)} %broadcast_in_dim.12.own_gain_ref.other_gain_ref, ...), custom_call_target="tpu_custom_call" | custom-call | flops 7516192768 | bytes 16777216 | tf_op jit(solution)/shard_map/project_tokens/pallas_call | solution.py:114
  35.2 1.3 pick.3
  36.6 10.8 %depthwise.1 = f32[1024,768]{1,0:T(8,128)S(1)} custom-call(bf16[1024,768]{1,0:T(8,128)(2,1)S(1)} %get-tuple-element.33.rows_ref, bf16[31,768]{1,0:T(8,128)(2,1)S(1)} %copy-done.7), custom_call_target="tpu_custom_call" | custom-call | flops 8589934592 | bytes 5242880 | tf_op jit(solution)/shard_map/depthwise/pallas_call | solution.py:235
  47.4 13.6 %collective-permute-done.refs_1_ = bf16[16,64,512]{2,1,0:T(8,128)(2,1)} collective-permute-done((bf16[16,64,512]{2,1,0:T(8,128)(2,1)}, bf16[16,64,512]{2,1,0:T(8,128)(2,1)}, u32[]{:S(2)}, u32[]{:S(2)}) %collective-permute-start) | collective-permute-done | bytes 1048608 | tf_op jit(solution)/shard_map/ppermute | solution.py:367
  62.4 1.7 %pick.4 = (bf16[8,64,512]{2,1,0:T(8,128)(2,1)S(1)}, bf16[8,64,512]{2,1,0:T(8,128)(2,1)S(1)}, bf16[8,64,512]{2,1,0:T(8,128)(2,1)S(1)}, bf16[8,64,512]{2,1,0:T(8,128)(2,1)S(1)}) custom-call(s32[4,16]{1,0:T(4,128)S(1)} %pad_add_fusion.refs_0_, bf16[16,64,512]{2,1,0:T(8,128)(2,1)} %collective-permute-done.refs_1_, ...), custom_call_target="tpu_custom_call" | custom-call | flops 268435456 | bytes 2097152 | tf_op jit(solution)/shard_map/pick/pallas_call | solution.py:192
  66.8 1.2 collective-permute-start.10
  68.2 1.3 collective-permute-start.13
  70.5 3.6 %collective-permute-done.7.refs_1_ = bf16[4,64,512]{2,1,0:T(8,128)(2,1)S(1)} collective-permute-done((bf16[4,64,512]{2,1,0:T(8,128)(2,1)S(1)}, bf16[4,64,512]{2,1,0:T(8,128)(2,1)S(1)}, u32[]{:S(2)}, u32[]{:S(2)}) %collective-permute-start.7) | collective-permute-done | bytes 262176 | tf_op jit(solution)/shard_map/ppermute | solution.py:363
  74.4 7.2 %collective-permute-done.14.refs_2_ = bf16[8,64,512]{2,1,0:T(8,128)(2,1)S(1)} collective-permute-done((bf16[8,64,512]{2,1,0:T(8,128)(2,1)S(1)}, bf16[8,64,512]{2,1,0:T(8,128)(2,1)S(1)}, u32[]{:S(2)}, u32[]{:S(2)}) %collective-permute-start.14) | collective-permute-done | bytes 524320 | tf_op jit(solution)/shard_map/ppermute | solution.py:367
  81.5 1.3 collective-permute-start.11
  82.8 9.4 %collective-permute-done.13.refs_1_ = bf16[8,64,512]{2,1,0:T(8,128)(2,1)S(1)} collective-permute-done((bf16[8,64,512]{2,1,0:T(8,128)(2,1)S(1)}, bf16[8,64,512]{2,1,0:T(8,128)(2,1)S(1)}, u32[]{:S(2)}, u32[]{:S(2)}) %collective-permute-start.13) | collective-permute-done | bytes 524320 | tf_op jit(solution)/shard_map/ppermute | solution.py:367
  92.2 1.2 collective-permute-start.12
  93.4 1.8 %fusion = f32[512,2048]{1,0:T(8,128)S(1)} fusion(bf16[768,2048]{1,0:T(8,128)(2,1)S(1)} %copy-done, bf16[1024,768]{1,0:T(8,128)(2,1)S(1)} %multiply_convert_fusion, s32[]{:T(128)S(6)} %select_n.76), kind=kOutput, calls=%fused_computation.5 | convolution fusion | flops 1610612736 | bytes 8126468 | tf_op jit(solution)/shard_map/dot_general | solution.py:39
  96.3 1.3 collective-permute-start.15
  97.8 1.2 collective-permute-start.17
  99.0 4.7 %collective-permute-done.12.refs_7_ = bf16[8,64,512]{2,1,0:T(8,128)(2,1)S(1)} collective-permute-done((bf16[8,64,512]{2,1,0:T(8,128)(2,1)S(1)}, bf16[8,64,512]{2,1,0:T(8,128)(2,1)S(1)}, u32[]{:S(2)}, u32[]{:S(2)}) %collective-permute-start.12) | collective-permute-done | bytes 524320 | tf_op jit(solution)/shard_map/ppermute | solution.py:363
  103.8 6.6 %collective-permute-done.15.refs_9_ = bf16[4,64,512]{2,1,0:T(8,128)(2,1)S(1)} collective-permute-done((bf16[4,64,512]{2,1,0:T(8,128)(2,1)S(1)}, bf16[4,64,512]{2,1,0:T(8,128)(2,1)S(1)}, u32[]{:S(2)}, u32[]{:S(2)}) %collective-permute-start.15) | collective-permute-done | bytes 262176 | tf_op jit(solution)/shard_map/ppermute | solution.py:363
  110.4 5.2 %collective-permute-done.16.refs_10_ = bf16[4,64,512]{2,1,0:T(8,128)(2,1)S(1)} collective-permute-done((bf16[4,64,512]{2,1,0:T(8,128)(2,1)S(1)}, bf16[4,64,512]{2,1,0:T(8,128)(2,1)S(1)}, u32[]{:S(2)}, u32[]{:S(2)}) %collective-permute-start.16) | collective-permute-done | bytes 262176 | tf_op jit(solution)/shard_map/ppermute | solution.py:363
  115.6 5.6 %attend.1 = bf16[1024,256]{1,0:T(8,128)(2,1)S(1)} custom-call(s32[32]{0:T(128)S(1)} %multiply_add_fusion.slots_ref, bf16[1024,256]{1,0:T(8,128)(2,1)S(1)} %get-tuple-element.35.query_ref, bf16[1,256]{1,0:T(2,128)(2,1)S(1)} %broadcast_in_dim.14.gate_ref, bf16[4,64,512]{2,1,0:T(8,128)(2,1)S(1)} %get-tuple-element.36.refs_0_, ...), custom_call_target="tpu_custom_call" | custom-call | flops 536870912 | bytes 5242880 | tf_op jit(solution)/shard_map/attend/pallas_call | solution.py:301
  122.7 1.9 %add_convert_fusion.1 = bf16[512,2048]{1,0:T(8,128)(2,1)} fusion(f32[512,2048]{1,0:T(8,128)S(1)} %fusion, f32[512,2048]{1,0:T(8,128)S(1)} %fusion.4), kind=kLoop, calls=%fused_computation.1 | loop fusion | flops 2097152 | bytes 10485760 | tf_op jit(solution)/shard_map/convert_element_type | solution.py:447
  124.6 8.7 %collective-permute-start.18 = (bf16[512,2048]{1,0:T(8,128)(2,1)}, bf16[512,2048]{1,0:T(8,128)(2,1)}, u32[]{:S(2)}, u32[]{:S(2)}) collective-permute-start(bf16[512,2048]{1,0:T(8,128)(2,1)} %add_convert_fusion.1), channel_id=1, source_target_pairs={{0,1},{1,0},{2,3},{3,2},{4,5},{5,4},{6,7},{7,6},{8,9},{9,8},{10,11... | collective-permute-start | bytes 6291464 | tf_op jit(solution)/shard_map/ppermute | solution.py:448
  133.4 3.0 %fusion.2 = f32[512,2048]{1,0:T(8,128)S(1)} fusion(bf16[768,2048]{1,0:T(8,128)(2,1)S(1)} %copy-done, bf16[1024,768]{1,0:T(8,128)(2,1)} %copy-done.10, s32[]{:T(128)S(6)} %select_n.75), kind=kOutput, calls=%fused_computation.7 | convolution fusion | flops 1610612736 | bytes 8126468 | tf_op jit(solution)/shard_map/dot_general | solution.py:39
  137.5 3.7 %add_convert_fusion = bf16[512,2048]{1,0:T(8,128)(2,1)} fusion(bf16[512,2048]{1,0:T(8,128)(2,1)} %collective-permute-done.18, bf16[512,2048]{1,0:T(8,128)(2,1)S(1)} %add_convert_fusion.2), kind=kLoop, calls=%fused_computation | loop fusion | flops 4194304 | bytes 6291456 | tf_op jit(solution)/shard_map/convert_element_type | solution.py:451
  (78 shorter events, 13.3 us)
Async XLA Ops:
  0.0 93.4 %copy-start = (bf16[768,2048]{1,0:T(8,128)(2,1)S(1)}, bf16[768,2048]{1,0:T(8,128)(2,1)}, u32[]{:S(2)}) copy-start(bf16[768,2048]{1,0:T(8,128)(2,1)} %param.32) | copy-start | bytes 9437188
  0.0 19.9 %collective-permute-start.5 = (bf16[1024,1024]{1,0:T(8,128)(2,1)}, bf16[1024,1024]{1,0:T(8,128)(2,1)}, u32[]{:S(2)}, u32[]{:S(2)}) collective-permute-start(bf16[1024,1024]{1,0:T(8,128)(2,1)} %own_ref.1), channel_id=1, source_target_pairs={{0,1},{1,0},{2,3},{3,2},{4,5},{5,4},{6,7},{7,6},{8,9},{9,8},{10,11... | collective-permute-start | bytes 6291464 | tf_op jit(solution)/shard_map/ppermute | solution.py:369
  2.3 1.2 copy-start.4
  4.7 8.2 %copy-start.13 = (s32[16,2]{0,1:T(2,128)S(1)}, s32[16,2]{0,1:T(2,128)}, u32[]{:S(2)}) copy-start(s32[16,2]{0,1:T(2,128)} %param.18) | copy-start | bytes 388
  4.8 10.3 %copy-start.14 = (bf16[256]{0:T(256)(128)(2,1)S(1)}, bf16[256]{0:T(256)(128)(2,1)}, u32[]{:S(2)}) copy-start(bf16[256]{0:T(256)(128)(2,1)} %param.26) | copy-start | bytes 1540
  4.8 10.3 %copy-start.12 = (bf16[768]{0:T(1024)(128)(2,1)S(1)}, bf16[768]{0:T(1024)(128)(2,1)}, u32[]{:S(2)}) copy-start(bf16[768]{0:T(1024)(128)(2,1)} %param.24) | copy-start | bytes 4612
  4.8 10.4 %copy-start.11 = (bf16[2048]{0:T(1024)(128)(2,1)S(1)}, bf16[2048]{0:T(1024)(128)(2,1)}, u32[]{:S(2)}) copy-start(bf16[2048]{0:T(1024)(128)(2,1)} %param.20) | copy-start | bytes 12292
  11.4 36.0 %collective-permute-start.1 = (bf16[16,64,512]{2,1,0:T(8,128)(2,1)}, bf16[16,64,512]{2,1,0:T(8,128)(2,1)}, u32[]{:S(2)}, u32[]{:S(2)}) collective-permute-start(bf16[16,64,512]{2,1,0:T(8,128)(2,1)} %bitcast.1.refs_1_), channel_id=1, source_target_pairs={{0,24},{2,26},{4,28},{6,30},{8,0},{10,2},{12,4},{14,6},{16,8},{18,... | collective-permute-start | bytes 3145736 | tf_op jit(solution)/shard_map/ppermute | solution.py:367
  11.6 49.4 %collective-permute-start = (bf16[16,64,512]{2,1,0:T(8,128)(2,1)}, bf16[16,64,512]{2,1,0:T(8,128)(2,1)}, u32[]{:S(2)}, u32[]{:S(2)}) collective-permute-start(bf16[16,64,512]{2,1,0:T(8,128)(2,1)} %bitcast.1.refs_1_), channel_id=1, source_target_pairs={{0,8},{2,10},{4,12},{6,14},{8,16},{10,18},{12,20},{14,22},{16,24},... | collective-permute-start | bytes 3145736 | tf_op jit(solution)/shard_map/ppermute | solution.py:367
  13.5 3.4 %collective-permute-start.4 = (s32[4,4]{1,0:T(4,128)S(1)}, s32[4,4]{1,0:T(4,128)S(1)}, u32[]{:S(2)}, u32[]{:S(2)}) collective-permute-start(s32[4,4]{1,0:T(4,128)S(1)} %bitcast.23), channel_id=1, source_target_pairs={{6,0},{4,2},{2,4},{0,6},{14,8},{12,10},{10,12},{8,14},{22,16},{20,... | collective-permute-start | bytes 200 | tf_op jit(solution)/shard_map/ppermute | solution.py:363
  13.8 3.5 %collective-permute-start.3 = (s32[4,4]{1,0:T(4,128)S(1)}, s32[4,4]{1,0:T(4,128)S(1)}, u32[]{:S(2)}, u32[]{:S(2)}) collective-permute-start(s32[4,4]{1,0:T(4,128)S(1)} %bitcast.22), channel_id=1, source_target_pairs={{4,0},{6,2},{0,4},{2,6},{12,8},{14,10},{8,12},{10,14},{20,16},{22,... | collective-permute-start | bytes 200 | tf_op jit(solution)/shard_map/ppermute | solution.py:363
  16.9 2.8 %collective-permute-start.2 = (s32[4,4]{1,0:T(4,128)S(1)}, s32[4,4]{1,0:T(4,128)S(1)}, u32[]{:S(2)}, u32[]{:S(2)}) collective-permute-start(s32[4,4]{1,0:T(4,128)S(1)} %bitcast.21), channel_id=1, source_target_pairs={{2,0},{0,2},{6,4},{4,6},{10,8},{8,10},{14,12},{12,14},{18,16},{16,... | collective-permute-start | bytes 200 | tf_op jit(solution)/shard_map/ppermute | solution.py:363
  19.9 1.6 %copy-start.3 = (bf16[1024,1024]{1,0:T(8,128)(2,1)S(1)}, bf16[1024,1024]{1,0:T(8,128)(2,1)}, u32[]{:S(2)}) copy-start(bf16[1024,1024]{1,0:T(8,128)(2,1)} %own_ref.1) | copy-start | bytes 6291460
  22.7 13.8 %copy-start.7 = (bf16[31,768]{1,0:T(8,128)(2,1)S(1)}, bf16[31,768]{1,0:T(8,128)(2,1)}, u32[]{:S(2)}) copy-start(bf16[31,768]{1,0:T(8,128)(2,1)} %taps_ref.1) | copy-start | bytes 142852
  61.5 6.7 %collective-permute-start.6 = (f32[2,1024]{1,0:T(2,128)S(1)}, f32[2,1024]{1,0:T(2,128)S(1)}, u32[]{:S(2)}, u32[]{:S(2)}) collective-permute-start(f32[2,1024]{1,0:T(2,128)S(1)} %pad_maximum_fusion), channel_id=1, source_target_pairs={{0,1},{1,0},{2,3},{3,2},{4,5},{5,4},{6,7},{7,6},{8,9},{9,8},{10,11... | collective-permute-start | bytes 24584 | tf_op jit(solution)/shard_map/ppermute | solution.py:427
  66.3 7.9 %collective-permute-start.7 = (bf16[4,64,512]{2,1,0:T(8,128)(2,1)S(1)}, bf16[4,64,512]{2,1,0:T(8,128)(2,1)S(1)}, u32[]{:S(2)}, u32[]{:S(2)}) collective-permute-start(bf16[4,64,512]{2,1,0:T(8,128)(2,1)S(1)} %get-tuple-element.37), channel_id=1, source_target_pairs={{0,2},{2,0},{4,6},{6,4},{8,10},{10,8},{12,14},{14,12},{16,18},{18,... | collective-permute-start | bytes 786440 | tf_op jit(solution)/shard_map/ppermute | solution.py:363
  66.6 29.7 %collective-permute-start.8 = (bf16[4,64,512]{2,1,0:T(8,128)(2,1)S(1)}, bf16[4,64,512]{2,1,0:T(8,128)(2,1)S(1)}, u32[]{:S(2)}, u32[]{:S(2)}) collective-permute-start(bf16[4,64,512]{2,1,0:T(8,128)(2,1)S(1)} %get-tuple-element.38), channel_id=1, source_target_pairs={{0,4},{2,6},{4,0},{6,2},{8,12},{10,14},{12,8},{14,10},{16,20},{18,... | collective-permute-start | bytes 786440 | tf_op jit(solution)/shard_map/ppermute | solution.py:363
  66.8 31.0 %collective-permute-start.10 = (bf16[8,64,512]{2,1,0:T(8,128)(2,1)S(1)}, bf16[8,64,512]{2,1,0:T(8,128)(2,1)S(1)}, u32[]{:S(2)}, u32[]{:S(2)}) collective-permute-start(bf16[8,64,512]{2,1,0:T(8,128)(2,1)S(1)} %get-tuple-element.43), channel_id=1, source_target_pairs={{0,2},{2,0},{4,6},{6,4},{8,10},{10,8},{12,14},{14,12},{16,18},{18,... | collective-permute-start | bytes 1572872 | tf_op jit(solution)/shard_map/ppermute | solution.py:363
  68.0 13.5 %collective-permute-start.14 = (bf16[8,64,512]{2,1,0:T(8,128)(2,1)S(1)}, bf16[8,64,512]{2,1,0:T(8,128)(2,1)S(1)}, u32[]{:S(2)}, u32[]{:S(2)}) collective-permute-start(bf16[8,64,512]{2,1,0:T(8,128)(2,1)S(1)} %slice.31), channel_id=1, source_target_pairs={{0,24},{2,26},{4,28},{6,30},{8,0},{10,2},{12,4},{14,6},{16,8},{18,... | collective-permute-start | bytes 1572872 | tf_op jit(solution)/shard_map/ppermute | solution.py:367
  68.2 24.1 %collective-permute-start.13 = (bf16[8,64,512]{2,1,0:T(8,128)(2,1)S(1)}, bf16[8,64,512]{2,1,0:T(8,128)(2,1)S(1)}, u32[]{:S(2)}, u32[]{:S(2)}) collective-permute-start(bf16[8,64,512]{2,1,0:T(8,128)(2,1)S(1)} %slice.30), channel_id=1, source_target_pairs={{0,8},{2,10},{4,12},{6,14},{8,16},{10,18},{12,20},{14,22},{16,24},... | collective-permute-start | bytes 1572872 | tf_op jit(solution)/shard_map/ppermute | solution.py:367
  70.5 22.9 %copy-start.10 = (bf16[1024,768]{1,0:T(8,128)(2,1)}, bf16[1024,768]{1,0:T(8,128)(2,1)S(1)}, u32[]{:S(2)}) copy-start(bf16[1024,768]{1,0:T(8,128)(2,1)S(1)} %multiply_convert_fusion) | copy-start | bytes 4718596
  74.2 23.4 %collective-permute-start.9 = (bf16[4,64,512]{2,1,0:T(8,128)(2,1)S(1)}, bf16[4,64,512]{2,1,0:T(8,128)(2,1)S(1)}, u32[]{:S(2)}, u32[]{:S(2)}) collective-permute-start(bf16[4,64,512]{2,1,0:T(8,128)(2,1)S(1)} %get-tuple-element.39), channel_id=1, source_target_pairs={{0,6},{2,4},{4,2},{6,0},{8,14},{10,12},{12,10},{14,8},{16,22},{18,... | collective-permute-start | bytes 786440 | tf_op jit(solution)/shard_map/ppermute | solution.py:363
  81.5 17.5 %collective-permute-start.11 = (bf16[8,64,512]{2,1,0:T(8,128)(2,1)S(1)}, bf16[8,64,512]{2,1,0:T(8,128)(2,1)S(1)}, u32[]{:S(2)}, u32[]{:S(2)}) collective-permute-start(bf16[8,64,512]{2,1,0:T(8,128)(2,1)S(1)} %get-tuple-element.44), channel_id=1, source_target_pairs={{0,4},{2,6},{4,0},{6,2},{8,12},{10,14},{12,8},{14,10},{16,20},{18,... | collective-permute-start | bytes 1572872 | tf_op jit(solution)/shard_map/ppermute | solution.py:363
  92.2 6.8 %copy-start.15 = (bf16[256]{0:T(256)(128)(2,1)S(1)}, bf16[256]{0:T(256)(128)(2,1)}, u32[]{:S(2)}) copy-start(bf16[256]{0:T(256)(128)(2,1)} %param.31) | copy-start | bytes 1540
  92.2 11.6 %collective-permute-start.12 = (bf16[8,64,512]{2,1,0:T(8,128)(2,1)S(1)}, bf16[8,64,512]{2,1,0:T(8,128)(2,1)S(1)}, u32[]{:S(2)}, u32[]{:S(2)}) collective-permute-start(bf16[8,64,512]{2,1,0:T(8,128)(2,1)S(1)} %get-tuple-element.45), channel_id=1, source_target_pairs={{0,6},{2,4},{4,2},{6,0},{8,14},{10,12},{12,10},{14,8},{16,22},{18,... | collective-permute-start | bytes 1572872 | tf_op jit(solution)/shard_map/ppermute | solution.py:363
  95.2 26.7 %copy-start.8 = (bf16[256,2048]{1,0:T(8,128)(2,1)S(1)}, bf16[256,2048]{1,0:T(8,128)(2,1)}, u32[]{:S(2)}) copy-start(bf16[256,2048]{1,0:T(8,128)(2,1)} %param.33) | copy-start | bytes 3145732
  96.3 14.1 %collective-permute-start.15 = (bf16[4,64,512]{2,1,0:T(8,128)(2,1)S(1)}, bf16[4,64,512]{2,1,0:T(8,128)(2,1)S(1)}, u32[]{:S(2)}, u32[]{:S(2)}) collective-permute-start(bf16[4,64,512]{2,1,0:T(8,128)(2,1)S(1)} %get-tuple-element.49), channel_id=1, source_target_pairs={{0,2},{2,0},{4,6},{6,4},{8,10},{10,8},{12,14},{14,12},{16,18},{18,... | collective-permute-start | bytes 786440 | tf_op jit(solution)/shard_map/ppermute | solution.py:363
  97.6 18.0 %collective-permute-start.16 = (bf16[4,64,512]{2,1,0:T(8,128)(2,1)S(1)}, bf16[4,64,512]{2,1,0:T(8,128)(2,1)S(1)}, u32[]{:S(2)}, u32[]{:S(2)}) collective-permute-start(bf16[4,64,512]{2,1,0:T(8,128)(2,1)S(1)} %get-tuple-element.50), channel_id=1, source_target_pairs={{0,4},{2,6},{4,0},{6,2},{8,12},{10,14},{12,8},{14,10},{16,20},{18,... | collective-permute-start | bytes 786440 | tf_op jit(solution)/shard_map/ppermute | solution.py:363
  97.8 17.8 %collective-permute-start.17 = (bf16[4,64,512]{2,1,0:T(8,128)(2,1)S(1)}, bf16[4,64,512]{2,1,0:T(8,128)(2,1)S(1)}, u32[]{:S(2)}, u32[]{:S(2)}) collective-permute-start(bf16[4,64,512]{2,1,0:T(8,128)(2,1)S(1)} %get-tuple-element.51), channel_id=1, source_target_pairs={{0,6},{2,4},{4,2},{6,0},{8,14},{10,12},{12,10},{14,8},{16,22},{18,... | collective-permute-start | bytes 786440 | tf_op jit(solution)/shard_map/ppermute | solution.py:363
  124.6 12.8 %collective-permute-start.18 = (bf16[512,2048]{1,0:T(8,128)(2,1)}, bf16[512,2048]{1,0:T(8,128)(2,1)}, u32[]{:S(2)}, u32[]{:S(2)}) collective-permute-start(bf16[512,2048]{1,0:T(8,128)(2,1)} %add_convert_fusion.1), channel_id=1, source_target_pairs={{0,1},{1,0},{2,3},{3,2},{4,5},{5,4},{6,7},{7,6},{8,9},{9,8},{10,11... | collective-permute-start | bytes 6291464 | tf_op jit(solution)/shard_map/ppermute | solution.py:448
  133.3 3.1 %copy-start.2 = (bf16[1024,256]{1,0:T(8,128)(2,1)S(1)}, bf16[1024,256]{1,0:T(8,128)(2,1)}, u32[]{:S(2)}) copy-start(bf16[1024,256]{1,0:T(8,128)(2,1)} %copy-done.1) | copy-start | bytes 1572868
  133.4 3.1 %copy-start.9 = (bf16[256,2048]{1,0:T(8,128)(2,1)S(1)}, bf16[256,2048]{1,0:T(8,128)(2,1)}, u32[]{:S(2)}) copy-start(bf16[256,2048]{1,0:T(8,128)(2,1)} %param.33) | copy-start | bytes 3145732
  (3 other events, 3.2 us)

commit v2 on v1

--- a/solution.py
+++ b/solution.py
@@ -15,7 +15,7 @@
 
 NORM_EPS = 1e-06
 LAYER_EPS = 1e-05
-VMEM_LIMIT = 48 * 1024 * 1024
+VMEM_LIMIT = 60 * 1024 * 1024
 
 
 def params():
@@ -48,16 +48,17 @@
     out_ref[:, width:] = dot32(normed, value_w_ref[...]).astype(jnp.bfloat16)
 
 
-def project_passages(rows, gain, key_weight, value_weight, key_gain):
-    count, features = rows.shape
+def project_passages(rows, start, count, gain, key_weight, value_weight, key_gain):
+    features = rows.shape[1]
     width = key_weight.shape[1]
     tile = min(256, count)
+    first = start // tile
     whole = lambda i: (0, 0)
     return pl.pallas_call(
         passage_kernel,
         grid=(count // tile,),
         in_specs=[
-            pl.BlockSpec((tile, features), lambda i: (i, 0)),
+            pl.BlockSpec((tile, features), lambda i: (i + first, 0)),
             pl.BlockSpec((1, features), whole),
             pl.BlockSpec((features, width), whole),
             pl.BlockSpec((features, width), whole),
@@ -161,36 +162,32 @@
     )
 
 
-def pick_kernel(most, stages, halves, *refs):
+def pick_kernel(most, stages, *refs):
     asked_ref, refs = refs[0], refs[1:]
-    count = halves if halves else len(stages)
-    blocks, outs = refs[:count], refs[count:]
+    blocks, outs = refs[: 2 * len(stages)], refs[2 * len(stages) :]
     for mate, out_ref in enumerate(outs):
         for place, relative in enumerate(stages):
+            low_ref, high_ref = blocks[2 * place], blocks[2 * place + 1]
+            split = low_ref.shape[0]
             for slot in range(most):
                 wanted = asked_ref[mate, relative * most + slot]
                 target = place * most + slot
-                if halves:
-                    split = blocks[0].shape[0]
-
-                    @pl.when(wanted < split)
-                    def _():
-                        out_ref[target] = blocks[0][jnp.minimum(wanted, split - 1)]
-
-                    @pl.when(wanted >= split)
-                    def _():
-                        out_ref[target] = blocks[1][jnp.maximum(wanted - split, 0)]
-
-                else:
-                    out_ref[target] = blocks[place][wanted]
-
-
-def pick(asked, blocks, stages, halves, most):
+
+                @pl.when(wanted < split)
+                def _(low_ref=low_ref, split=split, wanted=wanted, target=target):
+                    out_ref[target] = low_ref[jnp.minimum(wanted, split - 1)]
+
+                @pl.when(wanted >= split)
+                def _(high_ref=high_ref, split=split, wanted=wanted, target=target):
+                    out_ref[target] = high_ref[jnp.maximum(wanted - split, 0)]
+
+
+def pick(asked, blocks, stages, most):
     vmem = pl.BlockSpec(memory_space=pltpu.VMEM)
     mates = asked.shape[0]
     shape = (len(stages) * most,) + blocks[0].shape[1:]
     return pl.pallas_call(
-        functools.partial(pick_kernel, most, stages, len(blocks) if halves else 0),
+        functools.partial(pick_kernel, most, stages),
         in_specs=[pl.BlockSpec(memory_space=pltpu.SMEM)] + [vmem] * len(blocks),
         out_specs=[vmem] * mates,
         out_shape=[jax.ShapeDtypeStruct(shape, jnp.bfloat16)] * mates,
@@ -367,9 +364,20 @@
         return lax.ppermute(value, "st", pairs)
 
     other_tokens = lax.ppermute(tokens, "tp", swap)
-    own_block = project_passages(
-        passage_store.reshape(-1, feature_count), passage_gain, key_weight, value_weight, key_gain
-    ).reshape(store_size, passage_len, -1)
+    half = store_size // 2
+    store_rows = passage_store.reshape(-1, feature_count)
+    own_block = tuple(
+        project_passages(
+            store_rows,
+            start * passage_len,
+            half * passage_len,
+            passage_gain,
+            key_weight,
+            value_weight,
+            key_gain,
+        ).reshape(half, passage_len, -1)
+        for start in (0, half)
+    )
 
     flat_ids = passage_ids.reshape(-1)
     request_count = flat_ids.shape[0]
@@ -394,8 +402,8 @@
 
     pieces, plan = [], []
 
-    def deliver(blocks, stages, halves):
-        picked = pick(asked, blocks, stages, halves, most_each)
+    def deliver(blocks, stages):
+        picked = pick(asked, blocks, stages, most_each)
         for step, part in enumerate(picked):
             for place, offset in enumerate(stages):
                 plan.append(
@@ -414,15 +422,21 @@
         query_gain,
     )
     asked, gated_rows = lax.optimization_barrier((asked, gated_rows))
-    deliver((own_block,), (0,), False)
+    deliver(own_block, (0,))
     pieces[0], gated_rows = lax.optimization_barrier((pieces[0], gated_rows))
     filtered = depthwise(gated_rows, conv_weight, SEQS_DEV)
 
     rising, falling = own_block, own_block
     for hop in range(1, (depth - 1) // 2 + 1):
-        rising, falling = along_depth(rising, 1), along_depth(falling, -1)
-        rising, falling, filtered = lax.optimization_barrier((rising, falling, filtered))
-        deliver((rising, falling), (depth - hop, hop), False)
+        rising_low = along_depth(rising[0], 1)
+        falling_high = along_depth(falling[1], -1)
+        rising_high = along_depth(rising[1], 1)
+        falling_low = along_depth(falling[0], -1)
+        rising_high, falling_low, filtered = lax.optimization_barrier(
+            (rising_high, falling_low, filtered)
+        )
+        rising, falling = (rising_low, rising_high), (falling_low, falling_high)
+        deliver(rising + falling, (depth - hop, hop))
     own_sums = jnp.stack([jnp.sum(filtered, axis=-1), jnp.sum(filtered * filtered, axis=-1)])
     stat_sums = own_sums + lax.ppermute(own_sums, "tp", swap)
     channel_mean = (stat_sums[0] / C_A)[:, None]
@@ -435,10 +449,10 @@
     conv_send = dot32(lax.dynamic_slice_in_dim(conv_out, (1 - tp) * share, share), conv_out_weight)
     conv_keep = dot32(lax.dynamic_slice_in_dim(conv_out, tp * share, share), conv_out_weight)
     if depth % 2 == 0:
-        half = store_size // 2
-        low, high = along_depth(rising[:half], 1), along_depth(falling[half:], -1)
+        low = along_depth(rising[0], 1)
+        high = along_depth(falling[1], -1)
         low, high, conv_send = lax.optimization_barrier((low, high, conv_send))
-        deliver((low, high), (depth // 2,), True)
+        deliver((low, high), (depth // 2,))
 
     memory = attend(
         slot_index, queries, pieces, tuple(plan), most_each, memory_gate, passage_ids.shape[1]

time: 143 us -> 145 us (1.014)
  the two profiles are of different devices: /device:TPU:15 before, /device:TPU:0 now
where the time goes in v2:
time: 145 us
  waiting for transfers between devices  48.6 us (34%)
  Pallas kernels  44.1 us (30%)
  starting transfers between devices  29.9 us (21%)
  local copies, waits for them, and re-layouts  7.91 us (5%)
  other arithmetic  7.42 us (5%)
  matrix products  6.36 us (4%)
    ppermute x12, waiting for transfers between devices, along_plane(): lax.ppermute(value, 'st', [(b, a) for a, b in pairs] if back else pairs)  35 us
    ppermute x12, starting transfers between devices, along_plane(): lax.ppermute(value, 'st', [(b, a) for a, b in pairs] if back else pairs)  17.4 us
    pallas_call x1, Pallas kernels, project_tokens(): pl.pallas_call(token_kernel, grid_spec=pltpu.PrefetchScalarGridSpec(num_s...  13.6 us
    ppermute x6, waiting for transfers between devices, along_depth(): return lax.ppermute(value, 'st', pairs)  13 us
    ppermute x6, starting transfers between devices, along_depth(): return lax.ppermute(value, 'st', pairs)  12 us
    pallas_call x1, Pallas kernels, depthwise(): pl.pallas_call(conv_kernel, grid=(sequences, channels // width), in_specs...  10.7 us
    pallas_call x2, Pallas kernels, project_passages(): pl.pallas_call(passage_kernel, grid=(count // tile,), in_specs=[pl.BlockS...  9.56 us
    dot_general x4, matrix products, dot32(): return jnp.dot(left, right, preferred_element_type=jnp.float32)  6.36 us
  transfers between devices with their start and end apart: 21, of which 7 were waited for; matrix products, arithmetic and copies ran while one was open for 8% of the time, Pallas kernels for 27%

profile of v2, /device:TPU:0, one launch (start us, length us, event | category | flops | bytes accessed | tf_op | source)
XLA Modules:
  0.0 144.6 jit_solution(6671606782530765046)
XLA Ops:
  0.5 1.5 %broadcast_in_dim.11.key_gain_ref = bf16[1,256]{1,0:T(2,128)(2,1)} reshape(bf16[256]{0:T(256)(128)(2,1)} %param.30) | data formatting | bytes 1024 | tf_op jit(solution)/shard_map/broadcast_in_dim | solution.py:74
  3.3 4.8 %project_passages.2 = bf16[512,512]{1,0:T(8,128)(2,1)} custom-call(bf16[1024,2048]{1,0:T(8,128)(2,1)} %bitcast.21, bf16[1,2048]{1,0:T(2,128)(2,1)} %broadcast_in_dim.10.gain_ref, bf16[2048,256]{1,0:T(8,128)(2,1)} %key_w_ref.3, bf16[2048,256]{1,0:T(8,128)(2,1)} %value_w_ref.3, bf16[1,256]{1,0:T(2,128)(2,1)} %broadcast_in_dim.11.key_gain_ref), custom_call_target="tpu_custom_call" | custom-call | flops 1073741824 | bytes 8388608 | tf_op jit(solution)/shard_map/project_passages/pallas_call | solution.py:57
  8.1 4.6 %collective-permute-start.11 = (bf16[8,64,512]{2,1,0:T(8,128)(2,1)}, bf16[8,64,512]{2,1,0:T(8,128)(2,1)}, u32[]{:S(2)}, u32[]{:S(2)}) collective-permute-start(bf16[8,64,512]{2,1,0:T(8,128)(2,1)} %bitcast.15), channel_id=1, source_target_pairs={{0,24},{2,26},{4,28},{6,30},{8,0},{10,2},{12,4},{14,6},{16,8},{18,... | collective-permute-start | bytes 1572872 | tf_op jit(solution)/shard_map/ppermute | solution.py:364
  12.6 4.8 %project_passages.3 = bf16[512,512]{1,0:T(8,128)(2,1)} custom-call(bf16[1024,2048]{1,0:T(8,128)(2,1)} %bitcast.22, bf16[1,2048]{1,0:T(2,128)(2,1)} %broadcast_in_dim.10.gain_ref, bf16[2048,256]{1,0:T(8,128)(2,1)} %key_w_ref.3, bf16[2048,256]{1,0:T(8,128)(2,1)} %value_w_ref.3, bf16[1,256]{1,0:T(2,128)(2,1)} %broadcast_in_dim.11.key_gain_ref), custom_call_target="tpu_custom_call" | custom-call | flops 1073741824 | bytes 8388608 | tf_op jit(solution)/shard_map/project_passages/pallas_call | solution.py:57
  18.1 2.5 %collective-permute-start.4 = (s32[4,4]{1,0:T(4,128)S(1)}, s32[4,4]{1,0:T(4,128)S(1)}, u32[]{:S(2)}, u32[]{:S(2)}) collective-permute-start(s32[4,4]{1,0:T(4,128)S(1)} %bitcast.32), channel_id=1, source_target_pairs={{6,0},{4,2},{2,4},{0,6},{14,8},{12,10},{10,12},{8,14},{22,16},{20,... | collective-permute-start | bytes 200 | tf_op jit(solution)/shard_map/ppermute | solution.py:360
  22.6 1.5 %collective-permute-start.3 = (s32[4,4]{1,0:T(4,128)S(1)}, s32[4,4]{1,0:T(4,128)S(1)}, u32[]{:S(2)}, u32[]{:S(2)}) collective-permute-start(s32[4,4]{1,0:T(4,128)S(1)} %bitcast.31), channel_id=1, source_target_pairs={{4,0},{6,2},{0,4},{2,6},{12,8},{14,10},{8,12},{10,14},{20,16},{22,... | collective-permute-start | bytes 200 | tf_op jit(solution)/shard_map/ppermute | solution.py:360
  24.2 2.0 %collective-permute-done.3 = s32[4,4]{1,0:T(4,128)S(1)} collective-permute-done((s32[4,4]{1,0:T(4,128)S(1)}, s32[4,4]{1,0:T(4,128)S(1)}, u32[]{:S(2)}, u32[]{:S(2)}) %collective-permute-start.3) | collective-permute-done | bytes 96 | tf_op jit(solution)/shard_map/ppermute | solution.py:360
  26.2 1.5 %collective-permute-start.2 = (s32[4,4]{1,0:T(4,128)S(1)}, s32[4,4]{1,0:T(4,128)S(1)}, u32[]{:S(2)}, u32[]{:S(2)}) collective-permute-start(s32[4,4]{1,0:T(4,128)S(1)} %bitcast.30), channel_id=1, source_target_pairs={{2,0},{0,2},{6,4},{4,6},{10,8},{8,10},{14,12},{12,14},{18,16},{16,... | collective-permute-start | bytes 200 | tf_op jit(solution)/shard_map/ppermute | solution.py:360
  27.8 2.0 %collective-permute-done.2 = s32[4,4]{1,0:T(4,128)S(1)} collective-permute-done((s32[4,4]{1,0:T(4,128)S(1)}, s32[4,4]{1,0:T(4,128)S(1)}, u32[]{:S(2)}, u32[]{:S(2)}) %collective-permute-start.2) | collective-permute-done | bytes 96 | tf_op jit(solution)/shard_map/ppermute | solution.py:360
  29.8 3.8 %collective-permute-start.1 = (bf16[8,64,512]{2,1,0:T(8,128)(2,1)}, bf16[8,64,512]{2,1,0:T(8,128)(2,1)}, u32[]{:S(2)}, u32[]{:S(2)}) collective-permute-start(bf16[8,64,512]{2,1,0:T(8,128)(2,1)} %bitcast.19), channel_id=1, source_target_pairs={{0,24},{2,26},{4,28},{6,30},{8,0},{10,2},{12,4},{14,6},{16,8},{18,... | collective-permute-start | bytes 1572872 | tf_op jit(solution)/shard_map/ppermute | solution.py:364
  33.7 2.1 %collective-permute-start.16 = (bf16[8,64,512]{2,1,0:T(8,128)(2,1)}, bf16[8,64,512]{2,1,0:T(8,128)(2,1)}, u32[]{:S(2)}, u32[]{:S(2)}) collective-permute-start(bf16[8,64,512]{2,1,0:T(8,128)(2,1)} %collective-permute-done.11.refs_4_), channel_id=1, source_target_pairs={{0,24},{2,26},{4,28},{6,30},{8,0},{10,2},{12,4},{14,6},{16,8},{18,... | collective-permute-start | bytes 1572872 | tf_op jit(solution)/shard_map/ppermute | solution.py:364
  35.8 12.9 %collective-permute-done.10.refs_1_ = bf16[8,64,512]{2,1,0:T(8,128)(2,1)} collective-permute-done((bf16[8,64,512]{2,1,0:T(8,128)(2,1)}, bf16[8,64,512]{2,1,0:T(8,128)(2,1)}, u32[]{:S(2)}, u32[]{:S(2)}) %collective-permute-start.10) | collective-permute-done | bytes 524320 | tf_op jit(solution)/shard_map/ppermute | solution.py:364
  48.7 1.5 %collective-permute-start.15 = (bf16[8,64,512]{2,1,0:T(8,128)(2,1)}, bf16[8,64,512]{2,1,0:T(8,128)(2,1)}, u32[]{:S(2)}, u32[]{:S(2)}) collective-permute-start(bf16[8,64,512]{2,1,0:T(8,128)(2,1)} %collective-permute-done.10.refs_1_), channel_id=1, source_target_pairs={{0,8},{2,10},{4,12},{6,14},{8,16},{10,18},{12,20},{14,22},{16,24},... | collective-permute-start | bytes 1572872 | tf_op jit(solution)/shard_map/ppermute | solution.py:364
  50.3 13.6 %project_tokens.1 = (bf16[1024,768]{1,0:T(8,128)(2,1)}, bf16[1024,256]{1,0:T(8,128)(2,1)}) custom-call(s32[1]{0:T(128)} %bitcast.6.index_ref, bf16[1024,1024]{1,0:T(8,128)(2,1)} %own_ref.1, bf16[1024,1024]{1,0:T(8,128)(2,1)} %collective-permute-done.5.other_ref, bf16[1,2048]{1,0:T(2,128)(2,1)} %broadcast_in_dim.12.own_gain_ref.other_gain_ref, ...), custom_call_target="tpu_custom_call" | custom-call | flops 7516192768 | bytes 16777216 | tf_op jit(solution)/shard_map/project_tokens/pallas_call | solution.py:115
  65.8 1.6 %collective-permute-start.7 = (bf16[4,64,512]{2,1,0:T(8,128)(2,1)S(1)}, bf16[4,64,512]{2,1,0:T(8,128)(2,1)S(1)}, u32[]{:S(2)}, u32[]{:S(2)}) collective-permute-start(bf16[4,64,512]{2,1,0:T(8,128)(2,1)S(1)} %get-tuple-element.37), channel_id=1, source_target_pairs={{0,2},{2,0},{4,6},{6,4},{8,10},{10,8},{12,14},{14,12},{16,18},{18,... | collective-permute-start | bytes 786440 | tf_op jit(solution)/shard_map/ppermute | solution.py:360
  67.4 1.4 copy-done.7
  68.8 10.7 %depthwise.1 = f32[1024,768]{1,0:T(8,128)S(1)} custom-call(bf16[1024,768]{1,0:T(8,128)(2,1)S(1)} %copy-done.7, bf16[31,768]{1,0:T(8,128)(2,1)S(1)} %copy-done.6), custom_call_target="tpu_custom_call" | custom-call | flops 8589934592 | bytes 5242880 | tf_op jit(solution)/shard_map/depthwise/pallas_call | solution.py:232
  79.5 1.6 %collective-permute-start.8 = (bf16[4,64,512]{2,1,0:T(8,128)(2,1)S(1)}, bf16[4,64,512]{2,1,0:T(8,128)(2,1)S(1)}, u32[]{:S(2)}, u32[]{:S(2)}) collective-permute-start(bf16[4,64,512]{2,1,0:T(8,128)(2,1)S(1)} %get-tuple-element.38), channel_id=1, source_target_pairs={{0,4},{2,6},{4,0},{6,2},{8,12},{10,14},{12,8},{14,10},{16,20},{18,... | collective-permute-start | bytes 786440 | tf_op jit(solution)/shard_map/ppermute | solution.py:360
  81.6 2.1 %pick.4 = (bf16[8,64,512]{2,1,0:T(8,128)(2,1)S(1)}, bf16[8,64,512]{2,1,0:T(8,128)(2,1)S(1)}, bf16[8,64,512]{2,1,0:T(8,128)(2,1)S(1)}, bf16[8,64,512]{2,1,0:T(8,128)(2,1)S(1)}) custom-call(s32[4,16]{1,0:T(4,128)S(1)} %pad_add_fusion.refs_0_, bf16[8,64,512]{2,1,0:T(8,128)(2,1)} %collective-permute-done.10.refs_1_, ...), custom_call_target="tpu_custom_call" | custom-call | flops 268435456 | bytes 2097152 | tf_op jit(solution)/shard_map/pick/pallas_call | solution.py:189
  85.4 1.8 %fusion = f32[512,2048]{1,0:T(8,128)S(1)} fusion(bf16[768,2048]{1,0:T(8,128)(2,1)S(1)} %copy-done, bf16[1024,768]{1,0:T(8,128)(2,1)S(1)} %multiply_convert_fusion, s32[]{:T(128)S(6)} %select_n.76), kind=kOutput, calls=%fused_computation.5 | convolution fusion | flops 1610612736 | bytes 8126468 | tf_op jit(solution)/shard_map/dot_general | solution.py:39
  87.2 1.6 %collective-permute-start.12 = (bf16[8,64,512]{2,1,0:T(8,128)(2,1)S(1)}, bf16[8,64,512]{2,1,0:T(8,128)(2,1)S(1)}, u32[]{:S(2)}, u32[]{:S(2)}) collective-permute-start(bf16[8,64,512]{2,1,0:T(8,128)(2,1)S(1)} %get-tuple-element.43), channel_id=1, source_target_pairs={{0,2},{2,0},{4,6},{6,4},{8,10},{10,8},{12,14},{14,12},{16,18},{18,... | collective-permute-start | bytes 1572872 | tf_op jit(solution)/shard_map/ppermute | solution.py:360
  88.8 1.7 %pick.5 = (bf16[4,64,512]{2,1,0:T(8,128)(2,1)S(1)}, bf16[4,64,512]{2,1,0:T(8,128)(2,1)S(1)}, bf16[4,64,512]{2,1,0:T(8,128)(2,1)S(1)}, bf16[4,64,512]{2,1,0:T(8,128)(2,1)S(1)}) custom-call(s32[4,16]{1,0:T(4,128)S(1)} %pad_add_fusion.refs_0_, bf16[8,64,512]{2,1,0:T(8,128)(2,1)} %collective-permute-done.15.refs_1_, ...), custom_call_target="tpu_custom_call" | custom-call | flops 268435456 | bytes 2097152 | tf_op jit(solution)/shard_map/pick/pallas_call | solution.py:189
  91.1 1.5 %collective-permute-start.13 = (bf16[8,64,512]{2,1,0:T(8,128)(2,1)S(1)}, bf16[8,64,512]{2,1,0:T(8,128)(2,1)S(1)}, u32[]{:S(2)}, u32[]{:S(2)}) collective-permute-start(bf16[8,64,512]{2,1,0:T(8,128)(2,1)S(1)} %get-tuple-element.44), channel_id=1, source_target_pairs={{0,4},{2,6},{4,0},{6,2},{8,12},{10,14},{12,8},{14,10},{16,20},{18,... | collective-permute-start | bytes 1572872 | tf_op jit(solution)/shard_map/ppermute | solution.py:360
  92.6 1.4 collective-permute-start.14
  94.0 1.5 %collective-permute-start.18 = (bf16[4,64,512]{2,1,0:T(8,128)(2,1)S(1)}, bf16[4,64,512]{2,1,0:T(8,128)(2,1)S(1)}, u32[]{:S(2)}, u32[]{:S(2)}) collective-permute-start(bf16[4,64,512]{2,1,0:T(8,128)(2,1)S(1)} %get-tuple-element.50), channel_id=1, source_target_pairs={{0,4},{2,6},{4,0},{6,2},{8,12},{10,14},{12,8},{14,10},{16,20},{18,... | collective-permute-start | bytes 786440 | tf_op jit(solution)/shard_map/ppermute | solution.py:360
  95.5 14.3 %collective-permute-done.17.refs_9_ = bf16[4,64,512]{2,1,0:T(8,128)(2,1)S(1)} collective-permute-done((bf16[4,64,512]{2,1,0:T(8,128)(2,1)S(1)}, bf16[4,64,512]{2,1,0:T(8,128)(2,1)S(1)}, u32[]{:S(2)}, u32[]{:S(2)}) %collective-permute-start.17) | collective-permute-done | bytes 262176 | tf_op jit(solution)/shard_map/ppermute | solution.py:360
  109.8 1.5 %collective-permute-start.19 = (bf16[4,64,512]{2,1,0:T(8,128)(2,1)S(1)}, bf16[4,64,512]{2,1,0:T(8,128)(2,1)S(1)}, u32[]{:S(2)}, u32[]{:S(2)}) collective-permute-start(bf16[4,64,512]{2,1,0:T(8,128)(2,1)S(1)} %get-tuple-element.51), channel_id=1, source_target_pairs={{0,6},{2,4},{4,2},{6,0},{8,14},{10,12},{12,10},{14,8},{16,22},{18,... | collective-permute-start | bytes 786440 | tf_op jit(solution)/shard_map/ppermute | solution.py:360
  111.3 16.0 %collective-permute-done.18.refs_10_ = bf16[4,64,512]{2,1,0:T(8,128)(2,1)S(1)} collective-permute-done((bf16[4,64,512]{2,1,0:T(8,128)(2,1)S(1)}, bf16[4,64,512]{2,1,0:T(8,128)(2,1)S(1)}, u32[]{:S(2)}, u32[]{:S(2)}) %collective-permute-start.18) | collective-permute-done | bytes 262176 | tf_op jit(solution)/shard_map/ppermute | solution.py:360
  127.3 5.6 %attend.1 = bf16[1024,256]{1,0:T(8,128)(2,1)S(1)} custom-call(s32[32]{0:T(128)S(1)} %multiply_add_fusion.slots_ref, bf16[1024,256]{1,0:T(8,128)(2,1)S(1)} %copy-done.5, bf16[1,256]{1,0:T(2,128)(2,1)S(1)} %broadcast_in_dim.14.gate_ref, bf16[4,64,512]{2,1,0:T(8,128)(2,1)S(1)} %get-tuple-element.36.refs_0_, ...), custom_call_target="tpu_custom_call" | custom-call | flops 536870912 | bytes 5242880 | tf_op jit(solution)/shard_map/attend/pallas_call | solution.py:298
  134.4 1.9 %add_convert_fusion.1 = bf16[512,2048]{1,0:T(8,128)(2,1)} fusion(f32[512,2048]{1,0:T(8,128)S(1)} %fusion, f32[512,2048]{1,0:T(8,128)S(1)} %fusion.4), kind=kLoop, calls=%fused_computation.1 | loop fusion | flops 2097152 | bytes 10485760 | tf_op jit(solution)/shard_map/convert_element_type | solution.py:461
  136.4 3.0 %fusion.2 = f32[512,2048]{1,0:T(8,128)S(1)} fusion(bf16[768,2048]{1,0:T(8,128)(2,1)S(1)} %copy-done, bf16[1024,768]{1,0:T(8,128)(2,1)} %copy-done.10, s32[]{:T(128)S(6)} %select_n.75), kind=kOutput, calls=%fused_computation.7 | convolution fusion | flops 1610612736 | bytes 8126468 | tf_op jit(solution)/shard_map/dot_general | solution.py:39
  140.9 3.7 %add_convert_fusion = bf16[512,2048]{1,0:T(8,128)(2,1)} fusion(bf16[512,2048]{1,0:T(8,128)(2,1)} %collective-permute-done.20, bf16[512,2048]{1,0:T(8,128)(2,1)S(1)} %add_convert_fusion.2), kind=kLoop, calls=%fused_computation | loop fusion | flops 4194304 | bytes 6291456 | tf_op jit(solution)/shard_map/convert_element_type | solution.py:465
  (81 shorter events, 12.2 us)
Async XLA Ops:
  0.0 85.3 %copy-start = (bf16[768,2048]{1,0:T(8,128)(2,1)S(1)}, bf16[768,2048]{1,0:T(8,128)(2,1)}, u32[]{:S(2)}) copy-start(bf16[768,2048]{1,0:T(8,128)(2,1)} %param.32) | copy-start | bytes 9437188
  0.0 50.3 %collective-permute-start.5 = (bf16[1024,1024]{1,0:T(8,128)(2,1)}, bf16[1024,1024]{1,0:T(8,128)(2,1)}, u32[]{:S(2)}, u32[]{:S(2)}) collective-permute-start(bf16[1024,1024]{1,0:T(8,128)(2,1)} %own_ref.1), channel_id=1, source_target_pairs={{0,1},{1,0},{2,3},{3,2},{4,5},{5,4},{6,7},{7,6},{8,9},{9,8},{10,11... | collective-permute-start | bytes 6291464 | tf_op jit(solution)/shard_map/ppermute | solution.py:366
  8.0 9.4 %copy-start.13 = (s32[16,2]{0,1:T(2,128)S(1)}, s32[16,2]{0,1:T(2,128)}, u32[]{:S(2)}) copy-start(s32[16,2]{0,1:T(2,128)} %param.18) | copy-start | bytes 388
  8.0 12.6 %copy-start.14 = (bf16[256]{0:T(256)(128)(2,1)S(1)}, bf16[256]{0:T(256)(128)(2,1)}, u32[]{:S(2)}) copy-start(bf16[256]{0:T(256)(128)(2,1)} %param.26) | copy-start | bytes 1540
  8.0 13.2 %copy-start.12 = (bf16[768]{0:T(1024)(128)(2,1)S(1)}, bf16[768]{0:T(1024)(128)(2,1)}, u32[]{:S(2)}) copy-start(bf16[768]{0:T(1024)(128)(2,1)} %param.24) | copy-start | bytes 4612
  8.1 13.3 %copy-start.11 = (bf16[2048]{0:T(1024)(128)(2,1)S(1)}, bf16[2048]{0:T(1024)(128)(2,1)}, u32[]{:S(2)}) copy-start(bf16[2048]{0:T(1024)(128)(2,1)} %param.20) | copy-start | bytes 12292
  8.1 25.6 %collective-permute-start.11 = (bf16[8,64,512]{2,1,0:T(8,128)(2,1)}, bf16[8,64,512]{2,1,0:T(8,128)(2,1)}, u32[]{:S(2)}, u32[]{:S(2)}) collective-permute-start(bf16[8,64,512]{2,1,0:T(8,128)(2,1)} %bitcast.15), channel_id=1, source_target_pairs={{0,24},{2,26},{4,28},{6,30},{8,0},{10,2},{12,4},{14,6},{16,8},{18,... | collective-permute-start | bytes 1572872 | tf_op jit(solution)/shard_map/ppermute | solution.py:364
  12.6 66.9 %collective-permute-start = (bf16[8,64,512]{2,1,0:T(8,128)(2,1)}, bf16[8,64,512]{2,1,0:T(8,128)(2,1)}, u32[]{:S(2)}, u32[]{:S(2)}) collective-permute-start(bf16[8,64,512]{2,1,0:T(8,128)(2,1)} %bitcast.16), channel_id=1, source_target_pairs={{0,8},{2,10},{4,12},{6,14},{8,16},{10,18},{12,20},{14,22},{16,24},... | collective-permute-start | bytes 1572872 | tf_op jit(solution)/shard_map/ppermute | solution.py:364
  17.4 31.3 %collective-permute-start.10 = (bf16[8,64,512]{2,1,0:T(8,128)(2,1)}, bf16[8,64,512]{2,1,0:T(8,128)(2,1)}, u32[]{:S(2)}, u32[]{:S(2)}) collective-permute-start(bf16[8,64,512]{2,1,0:T(8,128)(2,1)} %bitcast.18), channel_id=1, source_target_pairs={{0,8},{2,10},{4,12},{6,14},{8,16},{10,18},{12,20},{14,22},{16,24},... | collective-permute-start | bytes 1572872 | tf_op jit(solution)/shard_map/ppermute | solution.py:364
  18.1 4.5 %collective-permute-start.4 = (s32[4,4]{1,0:T(4,128)S(1)}, s32[4,4]{1,0:T(4,128)S(1)}, u32[]{:S(2)}, u32[]{:S(2)}) collective-permute-start(s32[4,4]{1,0:T(4,128)S(1)} %bitcast.32), channel_id=1, source_target_pairs={{6,0},{4,2},{2,4},{0,6},{14,8},{12,10},{10,12},{8,14},{22,16},{20,... | collective-permute-start | bytes 200 | tf_op jit(solution)/shard_map/ppermute | solution.py:360
  22.6 3.6 %collective-permute-start.3 = (s32[4,4]{1,0:T(4,128)S(1)}, s32[4,4]{1,0:T(4,128)S(1)}, u32[]{:S(2)}, u32[]{:S(2)}) collective-permute-start(s32[4,4]{1,0:T(4,128)S(1)} %bitcast.31), channel_id=1, source_target_pairs={{4,0},{6,2},{0,4},{2,6},{12,8},{14,10},{8,12},{10,14},{20,16},{22,... | collective-permute-start | bytes 200 | tf_op jit(solution)/shard_map/ppermute | solution.py:360
  26.2 3.6 %collective-permute-start.2 = (s32[4,4]{1,0:T(4,128)S(1)}, s32[4,4]{1,0:T(4,128)S(1)}, u32[]{:S(2)}, u32[]{:S(2)}) collective-permute-start(s32[4,4]{1,0:T(4,128)S(1)} %bitcast.30), channel_id=1, source_target_pairs={{2,0},{0,2},{6,4},{4,6},{10,8},{8,10},{14,12},{12,14},{18,16},{16,... | collective-permute-start | bytes 200 | tf_op jit(solution)/shard_map/ppermute | solution.py:360
  29.8 51.3 %collective-permute-start.1 = (bf16[8,64,512]{2,1,0:T(8,128)(2,1)}, bf16[8,64,512]{2,1,0:T(8,128)(2,1)}, u32[]{:S(2)}, u32[]{:S(2)}) collective-permute-start(bf16[8,64,512]{2,1,0:T(8,128)(2,1)} %bitcast.19), channel_id=1, source_target_pairs={{0,24},{2,26},{4,28},{6,30},{8,0},{10,2},{12,4},{14,6},{16,8},{18,... | collective-permute-start | bytes 1572872 | tf_op jit(solution)/shard_map/ppermute | solution.py:364
  33.7 53.5 %collective-permute-start.16 = (bf16[8,64,512]{2,1,0:T(8,128)(2,1)}, bf16[8,64,512]{2,1,0:T(8,128)(2,1)}, u32[]{:S(2)}, u32[]{:S(2)}) collective-permute-start(bf16[8,64,512]{2,1,0:T(8,128)(2,1)} %collective-permute-done.11.refs_4_), channel_id=1, source_target_pairs={{0,24},{2,26},{4,28},{6,30},{8,0},{10,2},{12,4},{14,6},{16,8},{18,... | collective-permute-start | bytes 1572872 | tf_op jit(solution)/shard_map/ppermute | solution.py:364
  48.7 40.1 %collective-permute-start.15 = (bf16[8,64,512]{2,1,0:T(8,128)(2,1)}, bf16[8,64,512]{2,1,0:T(8,128)(2,1)}, u32[]{:S(2)}, u32[]{:S(2)}) collective-permute-start(bf16[8,64,512]{2,1,0:T(8,128)(2,1)} %collective-permute-done.10.refs_1_), channel_id=1, source_target_pairs={{0,8},{2,10},{4,12},{6,14},{8,16},{10,18},{12,20},{14,22},{16,24},... | collective-permute-start | bytes 1572872 | tf_op jit(solution)/shard_map/ppermute | solution.py:364
  50.3 13.7 %copy-start.3 = (bf16[512,512]{1,0:T(8,128)(2,1)S(1)}, bf16[512,512]{1,0:T(8,128)(2,1)}, u32[]{:S(2)}) copy-start(bf16[512,512]{1,0:T(8,128)(2,1)} %project_passages.2) | copy-start | bytes 1572868
  50.3 17.1 %copy-start.6 = (bf16[31,768]{1,0:T(8,128)(2,1)S(1)}, bf16[31,768]{1,0:T(8,128)(2,1)}, u32[]{:S(2)}) copy-start(bf16[31,768]{1,0:T(8,128)(2,1)} %taps_ref.1) | copy-start | bytes 142852
  65.8 25.3 %collective-permute-start.7 = (bf16[4,64,512]{2,1,0:T(8,128)(2,1)S(1)}, bf16[4,64,512]{2,1,0:T(8,128)(2,1)S(1)}, u32[]{:S(2)}, u32[]{:S(2)}) collective-permute-start(bf16[4,64,512]{2,1,0:T(8,128)(2,1)S(1)} %get-tuple-element.37), channel_id=1, source_target_pairs={{0,2},{2,0},{4,6},{6,4},{8,10},{10,8},{12,14},{14,12},{16,18},{18,... | collective-permute-start | bytes 786440 | tf_op jit(solution)/shard_map/ppermute | solution.py:360
  79.5 13.1 %collective-permute-start.8 = (bf16[4,64,512]{2,1,0:T(8,128)(2,1)S(1)}, bf16[4,64,512]{2,1,0:T(8,128)(2,1)S(1)}, u32[]{:S(2)}, u32[]{:S(2)}) collective-permute-start(bf16[4,64,512]{2,1,0:T(8,128)(2,1)S(1)} %get-tuple-element.38), channel_id=1, source_target_pairs={{0,4},{2,6},{4,0},{6,2},{8,12},{10,14},{12,8},{14,10},{16,20},{18,... | collective-permute-start | bytes 786440 | tf_op jit(solution)/shard_map/ppermute | solution.py:360
  81.5 2.2 %collective-permute-start.6 = (f32[2,1024]{1,0:T(2,128)S(1)}, f32[2,1024]{1,0:T(2,128)S(1)}, u32[]{:S(2)}, u32[]{:S(2)}) collective-permute-start(f32[2,1024]{1,0:T(2,128)S(1)} %pad_maximum_fusion), channel_id=1, source_target_pairs={{0,1},{1,0},{2,3},{3,2},{4,5},{5,4},{6,7},{7,6},{8,9},{9,8},{10,11... | collective-permute-start | bytes 24584 | tf_op jit(solution)/shard_map/ppermute | solution.py:441
  83.7 10.3 %collective-permute-start.9 = (bf16[4,64,512]{2,1,0:T(8,128)(2,1)S(1)}, bf16[4,64,512]{2,1,0:T(8,128)(2,1)S(1)}, u32[]{:S(2)}, u32[]{:S(2)}) collective-permute-start(bf16[4,64,512]{2,1,0:T(8,128)(2,1)S(1)} %get-tuple-element.39), channel_id=1, source_target_pairs={{0,6},{2,4},{4,2},{6,0},{8,14},{10,12},{12,10},{14,8},{16,22},{18,... | collective-permute-start | bytes 786440 | tf_op jit(solution)/shard_map/ppermute | solution.py:360
  85.3 26.0 %copy-start.15 = (bf16[256]{0:T(256)(128)(2,1)S(1)}, bf16[256]{0:T(256)(128)(2,1)}, u32[]{:S(2)}) copy-start(bf16[256]{0:T(256)(128)(2,1)} %param.31) | copy-start | bytes 1540
  85.3 42.0 %copy-start.5 = (bf16[1024,256]{1,0:T(8,128)(2,1)S(1)}, bf16[1024,256]{1,0:T(8,128)(2,1)}, u32[]{:S(2)}) copy-start(bf16[1024,256]{1,0:T(8,128)(2,1)} %get-tuple-element.35.query_ref) | copy-start | bytes 1572868
  87.2 46.5 %copy-start.8 = (bf16[256,2048]{1,0:T(8,128)(2,1)S(1)}, bf16[256,2048]{1,0:T(8,128)(2,1)}, u32[]{:S(2)}) copy-start(bf16[256,2048]{1,0:T(8,128)(2,1)} %param.33) | copy-start | bytes 3145732
  87.2 40.1 %collective-permute-start.12 = (bf16[8,64,512]{2,1,0:T(8,128)(2,1)S(1)}, bf16[8,64,512]{2,1,0:T(8,128)(2,1)S(1)}, u32[]{:S(2)}, u32[]{:S(2)}) collective-permute-start(bf16[8,64,512]{2,1,0:T(8,128)(2,1)S(1)} %get-tuple-element.43), channel_id=1, source_target_pairs={{0,2},{2,0},{4,6},{6,4},{8,10},{10,8},{12,14},{14,12},{16,18},{18,... | collective-permute-start | bytes 1572872 | tf_op jit(solution)/shard_map/ppermute | solution.py:360
  90.5 19.3 %collective-permute-start.17 = (bf16[4,64,512]{2,1,0:T(8,128)(2,1)S(1)}, bf16[4,64,512]{2,1,0:T(8,128)(2,1)S(1)}, u32[]{:S(2)}, u32[]{:S(2)}) collective-permute-start(bf16[4,64,512]{2,1,0:T(8,128)(2,1)S(1)} %get-tuple-element.49), channel_id=1, source_target_pairs={{0,2},{2,0},{4,6},{6,4},{8,10},{10,8},{12,14},{14,12},{16,18},{18,... | collective-permute-start | bytes 786440 | tf_op jit(solution)/shard_map/ppermute | solution.py:360
  91.1 36.2 %collective-permute-start.13 = (bf16[8,64,512]{2,1,0:T(8,128)(2,1)S(1)}, bf16[8,64,512]{2,1,0:T(8,128)(2,1)S(1)}, u32[]{:S(2)}, u32[]{:S(2)}) collective-permute-start(bf16[8,64,512]{2,1,0:T(8,128)(2,1)S(1)} %get-tuple-element.44), channel_id=1, source_target_pairs={{0,4},{2,6},{4,0},{6,2},{8,12},{10,14},{12,8},{14,10},{16,20},{18,... | collective-permute-start | bytes 1572872 | tf_op jit(solution)/shard_map/ppermute | solution.py:360
  92.6 34.7 %collective-permute-start.14 = (bf16[8,64,512]{2,1,0:T(8,128)(2,1)S(1)}, bf16[8,64,512]{2,1,0:T(8,128)(2,1)S(1)}, u32[]{:S(2)}, u32[]{:S(2)}) collective-permute-start(bf16[8,64,512]{2,1,0:T(8,128)(2,1)S(1)} %get-tuple-element.45), channel_id=1, source_target_pairs={{0,6},{2,4},{4,2},{6,0},{8,14},{10,12},{12,10},{14,8},{16,22},{18,... | collective-permute-start | bytes 1572872 | tf_op jit(solution)/shard_map/ppermute | solution.py:360
  94.0 33.3 %collective-permute-start.18 = (bf16[4,64,512]{2,1,0:T(8,128)(2,1)S(1)}, bf16[4,64,512]{2,1,0:T(8,128)(2,1)S(1)}, u32[]{:S(2)}, u32[]{:S(2)}) collective-permute-start(bf16[4,64,512]{2,1,0:T(8,128)(2,1)S(1)} %get-tuple-element.50), channel_id=1, source_target_pairs={{0,4},{2,6},{4,0},{6,2},{8,12},{10,14},{12,8},{14,10},{16,20},{18,... | collective-permute-start | bytes 786440 | tf_op jit(solution)/shard_map/ppermute | solution.py:360
  109.8 17.5 %collective-permute-start.19 = (bf16[4,64,512]{2,1,0:T(8,128)(2,1)S(1)}, bf16[4,64,512]{2,1,0:T(8,128)(2,1)S(1)}, u32[]{:S(2)}, u32[]{:S(2)}) collective-permute-start(bf16[4,64,512]{2,1,0:T(8,128)(2,1)S(1)} %get-tuple-element.51), channel_id=1, source_target_pairs={{0,6},{2,4},{4,2},{6,0},{8,14},{10,12},{12,10},{14,8},{16,22},{18,... | collective-permute-start | bytes 786440 | tf_op jit(solution)/shard_map/ppermute | solution.py:360
  136.4 4.5 %collective-permute-start.20 = (bf16[512,2048]{1,0:T(8,128)(2,1)}, bf16[512,2048]{1,0:T(8,128)(2,1)}, u32[]{:S(2)}, u32[]{:S(2)}) collective-permute-start(bf16[512,2048]{1,0:T(8,128)(2,1)} %add_convert_fusion.1), channel_id=1, source_target_pairs={{0,1},{1,0},{2,3},{3,2},{4,5},{5,4},{6,7},{7,6},{8,9},{9,8},{10,11... | collective-permute-start | bytes 6291464 | tf_op jit(solution)/shard_map/ppermute | solution.py:462
  136.4 3.1 %copy-start.9 = (bf16[256,2048]{1,0:T(8,128)(2,1)S(1)}, bf16[256,2048]{1,0:T(8,128)(2,1)}, u32[]{:S(2)}) copy-start(bf16[256,2048]{1,0:T(8,128)(2,1)} %param.33) | copy-start | bytes 3145732
  (5 other events, 8.2 us)
